TPU v7x, 256 devices: a whole 4x4x8 slice. The times are simulated.
256 devices in a mesh: ep: 16 (over y, x), tp: 16 (over z, core).
Axes of the slice: x: 4, y: 4, z: 8, core: 2. Of those that a mesh axis runs over, the one named last changes fastest.
Arguments:
- mix_in: bfloat16 [32768, 2048], P(('ep', 'tp')), may hold values from -6 to 6
- mix_gain: float32 [2048], replicated, may hold values from 0.1 to 1.9
- mix_w_in: bfloat16 [2048, 512], P('tp'), may hold values from -0.125 to 0.125
- pool_mat: bfloat16 [4, 128, 128], replicated, may hold values from -0.5 to 0.5
- pool_scale: float32 [512], replicated, may hold values from 0.1 to 1.9
- mix_w_out: bfloat16 [512, 2048], P(None, 'tp'), may hold values from -0.25 to 0.25
- moe_in: bfloat16 [32768, 2048], P(('ep', 'tp')), may hold values from -6 to 6
- moe_gain: float32 [2048], replicated, may hold values from 0.1 to 1.9
- routes: int32 [32768, 2], P('ep'), may hold values from 0 to 255, all different within a row; in each aligned block of 2048 rows (0 to 2047, 2048 to 4095, ...) at most 32 rows name the same one
- route_score: bfloat16 [32768, 2], P('ep'), may hold values from 0.099609375 to 1
- exp_gate: bfloat16 [256, 2048, 768], P(('ep', 'tp')), may hold values from -0.125 to 0.125
- exp_up: bfloat16 [256, 2048, 768], P(('ep', 'tp')), may hold values from -0.125 to 0.125
- exp_down: bfloat16 [256, 768, 2048], P(('ep', 'tp')), may hold values from -0.21875 to 0.21875
- shared_gate: bfloat16 [768, 2048], P('tp'), may hold values from -0.125 to 0.125
- shared_up: bfloat16 [768, 2048], P('tp'), may hold values from -0.125 to 0.125
- shared_down: bfloat16 [768, 2048], P('tp'), may hold values from -0.21875 to 0.21875
Outputs:
- mixed: bfloat16 [32768, 2048], P(('ep', 'tp'))
- moe_out: bfloat16 [32768, 2048], P(('ep', 'tp'))
Inputs may be any that keep to these rules, and one draw needn't show every extreme that they name: `routes`: each row names 2 different experts. Within the rows of one index of ep (aligned blocks of 2048 rows) no expert is named more than 32 times, a bound that some expert reaches in some blocks.
All inputs are finite; a program needn't handle non-finite values.
Results may differ from a plain program's by a relative error of at most 0.012.
Values may be sent and summed in bfloat16 or wider, within the bound.
A program may use at most 128 MiB of HBM per device.

v0:
```python
import jax
import jax.numpy as jnp
from jax import lax
from jax.sharding import PartitionSpec as P

SEQS_MIX = 1


NORM_EPS = 1e-06
ROUTED_SCALE = 2.5


def shifted(value, axis, steps):
    count = lax.axis_size(axis)
    first, last = (max(0, -steps), min(count, count - steps))
    return lax.ppermute(value, axis, [(source, source + steps) for source in range(first, last)])


def sent_together(arrays, axis, dim, along):
    widths = [a.shape[along] for a in arrays]
    both = jnp.concatenate(arrays, axis=along)
    whole = lax.all_gather(both, axis, axis=dim, tiled=True)
    return tuple(jnp.split(whole, [sum(widths[:k]) for k in range(1, len(widths))], axis=along))


def rms_rows(values, gain):
    floats = values.astype(jnp.float32)
    scaled = floats * lax.rsqrt(jnp.mean(floats * floats, axis=-1, keepdims=True) + NORM_EPS)
    return (scaled * gain).astype(jnp.bfloat16)


def expert_ffn(rows_in, w_gate, w_up, w_down):
    row_shape = rows_in.shape
    flat_rows = rows_in.reshape(-1, row_shape[-1])
    gate_act = jnp.dot(flat_rows, w_gate, preferred_element_type=jnp.float32)
    up_act = jnp.dot(flat_rows, w_up, preferred_element_type=jnp.float32)
    hidden = (jax.nn.silu(gate_act) * up_act).astype(jnp.bfloat16)
    outputs = jnp.dot(hidden, w_down, preferred_element_type=jnp.float32).astype(jnp.bfloat16)
    return outputs.reshape(row_shape)


def shared_hidden_rows(rows_in, w_gate, w_up):
    contract = (((1,), (1,)), ((), ()))
    gate_act = lax.dot_general(rows_in, w_gate, contract, preferred_element_type=jnp.float32)
    up_act = lax.dot_general(rows_in, w_up, contract, preferred_element_type=jnp.float32)
    return (jax.nn.silu(gate_act) * up_act).astype(jnp.bfloat16)


def pool_mix(projected, prior_tail, first_row, seq_len, pool_mat, pool_scale):
    tokens, channels = projected.shape
    groups = pool_mat.shape[0]
    group_ch = pool_mat.shape[1]
    reach_rows = prior_tail.shape[0]
    extended = jnp.concatenate([prior_tail, projected], axis=0).astype(jnp.float32)
    prefix = jnp.concatenate(
        [jnp.zeros((1, channels), jnp.float32), jnp.cumsum(extended, axis=0)], axis=0
    )
    position = (first_row + lax.iota(jnp.int32, tokens)) % seq_len
    pieces = []
    for group in range(groups):
        window_len = 2 ** (group + 1)
        lower = group * group_ch
        upper = lower + group_ch
        window_sum = (
            prefix[reach_rows + 1 : reach_rows + 1 + tokens, lower:upper]
            - prefix[
                reach_rows + 1 - window_len : reach_rows + 1 - window_len + tokens, lower:upper
            ]
        )
        counts = jnp.minimum(position + 1, window_len).astype(jnp.float32)
        pieces.append(window_sum / counts[:, None] - extended[reach_rows:, lower:upper])
    pooled = jnp.concatenate(pieces, axis=1).astype(jnp.bfloat16).reshape(tokens, groups, group_ch)
    grouped = jnp.einsum("tgc,gcd->tgd", pooled, pool_mat, preferred_element_type=jnp.float32)
    return (grouped.reshape(tokens, channels) * pool_scale).astype(jnp.bfloat16)


def mixer_half(mix_in, mix_gain, pool_mat, pool_scale, joint):
    normed = rms_rows(mix_in, mix_gain)
    tokens = normed.shape[0]
    projected = jnp.dot(normed, joint[0], preferred_element_type=jnp.float32).astype(jnp.bfloat16)
    groups = pool_mat.shape[0]
    reach_rows = 2**groups - 1
    devices = lax.axis_size("ep") * lax.axis_size("tp")
    seq_len = tokens * devices // SEQS_MIX
    first_row = lax.axis_index(("ep", "tp")) * tokens
    arrived = shifted(projected[tokens - reach_rows :], ("ep", "tp"), 1)
    prior_tail = jnp.where(first_row % seq_len == 0, jnp.zeros_like(arrived), arrived)
    pool_out = pool_mix(projected, prior_tail, first_row, seq_len, pool_mat, pool_scale)
    return jnp.dot(pool_out, joint[1], preferred_element_type=jnp.float32).astype(jnp.bfloat16)


def expert_half(
    rows_all, own_normed, routes, route_score, exp_gate, exp_up, exp_down, shared_weights
):
    block_rows, model_width = rows_all.shape
    top_count = routes.shape[1]
    ep_count = lax.axis_size("ep")
    tp_count = lax.axis_size("tp")
    column = lax.axis_index("tp")
    capacity = 2 * block_rows * top_count // (ep_count * tp_count)
    scores = route_score.astype(jnp.float32)
    weights = scores / jnp.sum(scores, axis=1, keepdims=True) * ROUTED_SCALE
    flat_expert = routes.reshape(-1)
    flat_weight = weights.reshape(-1)
    flat_token = lax.iota(jnp.int32, block_rows * top_count) // top_count
    owned_copy = flat_expert % tp_count == column
    target = flat_expert // tp_count
    onehot = (
        (target[:, None] == lax.iota(jnp.int32, ep_count)[None, :]) & owned_copy[:, None]
    ).astype(jnp.int32)
    before = jnp.sum((jnp.cumsum(onehot, axis=0) - onehot) * onehot, axis=1)
    slot_index = jnp.where(owned_copy, target * capacity + before, ep_count * capacity)
    slot_token = (
        jnp.full((ep_count * capacity,), block_rows, jnp.int32)
        .at[slot_index]
        .set(flat_token, mode="drop")
    )
    slot_weight = (
        jnp.zeros((ep_count * capacity,), jnp.float32).at[slot_index].set(flat_weight, mode="drop")
    )
    live_slot = (slot_token < block_rows).astype(jnp.bfloat16)
    outgoing = (
        jnp.take(rows_all, jnp.minimum(slot_token, block_rows - 1), axis=0) * live_slot[:, None]
    )
    outgoing = outgoing.reshape(ep_count, capacity, model_width)
    results = expert_ffn(
        lax.all_to_all(outgoing, "ep", split_axis=0, concat_axis=0, tiled=True),
        exp_gate[0],
        exp_up[0],
        exp_down[0],
    )
    returned = lax.all_to_all(results, "ep", split_axis=0, concat_axis=0, tiled=True)
    weighted = returned.reshape(-1, model_width).astype(jnp.float32) * slot_weight[:, None]
    routed = (
        jnp.zeros((block_rows, model_width), jnp.float32).at[slot_token].add(weighted, mode="drop")
    )
    routed_sum = lax.psum_scatter(
        routed.astype(jnp.bfloat16), "tp", scatter_dimension=0, tiled=True
    ).astype(jnp.float32)
    hidden_own = shared_hidden_rows(own_normed, shared_weights[0], shared_weights[1])
    shared_out = jnp.dot(hidden_own, shared_weights[2], preferred_element_type=jnp.float32)
    return (routed_sum + shared_out).astype(jnp.bfloat16)


def shards(
    mix_in,
    mix_gain,
    mix_w_in,
    pool_mat,
    pool_scale,
    mix_w_out,
    moe_in,
    moe_gain,
    routes,
    route_score,
    exp_gate,
    exp_up,
    exp_down,
    shared_gate,
    shared_up,
    shared_down,
):
    shared_weights = sent_together((shared_gate, shared_up, shared_down), "tp", 0, 1)
    moe_normed = rms_rows(moe_in, moe_gain)
    joint = (
        lax.all_gather(mix_w_in, "tp", axis=0, tiled=True),
        lax.all_gather(mix_w_out, "tp", axis=1, tiled=True),
        lax.all_gather(moe_normed, "tp", axis=0, tiled=True),
    )
    mixed = mixer_half(mix_in, mix_gain, pool_mat, pool_scale, joint)
    moe_out = expert_half(
        joint[2], moe_normed, routes, route_score, exp_gate, exp_up, exp_down, shared_weights
    )
    return (mixed, moe_out)


def solution(mesh):
    return jax.shard_map(
        shards,
        mesh=mesh,
        in_specs=(
            P(("ep", "tp"), None),
            P(),
            P("tp", None),
            P(),
            P(),
            P(None, "tp"),
            P(("ep", "tp"), None),
            P(),
            P("ep", None),
            P("ep", None),
            P(("ep", "tp"), None, None),
            P(("ep", "tp"), None, None),
            P(("ep", "tp"), None, None),
            P("tp", None),
            P("tp", None),
            P("tp", None),
        ),
        out_specs=(P(("ep", "tp"), None), P(("ep", "tp"), None)),
        check_vma=False,
    )
```

profile of v0, /device:TPU:2, one launch (start us, length us, event | category | flops | bytes accessed | tf_op | source)
XLA Modules:
  0.0 296.6 jit_solution(2736446346322186071)
XLA Ops:
  7.2 0.0 copy-start
  7.2 0.0 all-gather.9.cloned.1.call-start
  7.3 1.4 fusion.37
  8.6 2.0 fusion.39
  10.7 0.0 all-gather.9.cloned.1.call-update
  10.7 0.0 all-gather.5.cloned.1.call-start
  10.8 0.7 all-gather.5.cloned.1.call-update
  11.5 0.0 all-gather.7.cloned.1.call-start
  11.5 0.7 all-gather.7.cloned.1.call-update
  12.2 0.0 all-gather.11.cloned.1.call-start
  12.3 1.8 pad_maximum_fusion
  14.0 0.0 all-gather.11.cloned.1.call-update
  14.1 1.4 copy.24
  15.5 1.7 reshape.284
  17.2 1.7 reshape.283
  18.9 1.8 reshape.282
  20.8 0.7 fusion.58
  21.5 8.3 %reduce-window.16 = s32[16,32,128]{2,1,0:T(8,128)S(1)} reduce-window(s32[16,32,128]{2,1,0:T(8,128)} %fusion.58, s32[]{:T(128)} %constant.107.clone.1), window={size=1x1x128 pad=0_0x0_0x127_0}, to_apply=%region_3.4 | reduce-window | flops 8323072 | bytes 524292 | tf_op jit(solution)/shard_map/reduce-window.2
  29.8 0.5 slice_reduce_fusion
  30.3 0.2 reduce-window.19
  30.5 0.1 broadcast_add_fusion.1
  30.7 0.2 fusion.54
  30.9 0.1 compare_select_fusion
  31.0 15.5 %scatter_custom_fusion = s32[512]{0:T(512)S(1)} fusion(s32[4096]{0:T(1024)S(1)} %bitcast.87, s32[4096]{0:T(1024)S(1)} %add_select_fusion, s32[]{:T(128)} %constant.118.clone.1), kind=kCustom, calls=%fused_computation.142 | custom fusion | bytes 2052 | tf_op jit(solution)/shard_map/scatter | solution.py:116
  46.6 0.1 reshape.289
  46.6 0.1 broadcast_in_dim.52
  46.7 22.9 %all-gather.9.cloned.1.call-done = bf16[2048,2048]{1,0:T(8,128)(2,1)} async-done(((bf16[128,2048]{1,0:T(8,128)(2,1)}), bf16[2048,2048]{1,0:T(8,128)(2,1)}) %all-gather.9.cloned.1.call-update) | async-done | bytes 8388624 | tf_op jit(solution)/shard_map/all_gather | solution.py:168
  69.6 9.7 %gather_fusion = bf16[512,2048]{1,0:T(8,128)(2,1)} fusion(bf16[2048,2048]{1,0:T(8,128)(2,1)} %all-gather.9.cloned.1.call-done, s32[1024]{0:T(1024)S(1)} %pad_clamp_fusion), kind=kCustom, calls=%fused_computation | custom fusion | bytes 4196352 | tf_op jit(solution)/shard_map/jit(_take)/gather | solution.py:123
  79.3 1.9 select_multiply_fusion
  81.2 0.0 copy-start.10
  81.2 34.8 %all_to_all.10 = bf16[16,32,2048]{2,1,0:T(8,128)(2,1)S(1)} all-to-all(bf16[16,32,2048]{2,1,0:T(8,128)(2,1)S(1)} %select_multiply_fusion), channel_id=1, replica_groups=mesh['ep'=16,'tp'=16] {'ep'}, dimensions={0} | all-to-all | bytes 4194304 | tf_op jit(solution)/shard_map/all_to_all | solution.py:127
  116.0 1.3 copy-done.2
  117.3 3.0 fusion.12
  120.3 8.4 %fusion.14 = bf16[512,2048]{1,0:T(8,128)(2,1)} fusion(bf16[1,768,2048]{2,1,0:T(8,128)(2,1)S(1)} %copy-done, f32[512,768]{1,0:T(8,128)} %fusion.12, bf16[512,2048]{1,0:T(8,128)(2,1)} %bitcast.80, bf16[1,2048,768]{2,1,0:T(8,128)(2,1)} %param.27), kind=kOutput, calls=%fused_computation.19 | convolution fusion | flops 3224633344 | bytes 12058624 | tf_op jit(solution)/shard_map/dot_general | solution.py:38
  128.7 5.1 %all-to-all-start.1 = ((bf16[16,32,2048]{2,1,0:T(8,128)(2,1)}), bf16[16,32,2048]{2,1,0:T(8,128)(2,1)S(1)}, u32[]{:S(2)}, u32[]{:S(2)}) async-start(bf16[16,32,2048]{2,1,0:T(8,128)(2,1)} %bitcast.78), calls=%async_computation.1 | async-start | bytes 4194304 | tf_op jit(solution)/shard_map/all_to_all | solution.py:132
  133.7 0.0 reduce-scatter.2.cloned.1.call-start
  133.8 0.4 copy.27
  134.2 0.5 reshape.311
  134.7 15.7 %scatter_custom_fusion.1 = f32[512]{0:T(512)S(1)} fusion(s32[4096]{0:T(1024)S(1)} %bitcast.88, f32[4096]{0:T(1024)S(1)} %reshape.311, f32[]{:T(128)} %constant.111.clone.1), kind=kCustom, calls=%fused_computation.140 | custom fusion | bytes 2052 | tf_op jit(solution)/shard_map/scatter | solution.py:119
  150.4 9.9 %all-to-all-done.1 = bf16[16,32,2048]{2,1,0:T(8,128)(2,1)S(1)} async-done(((bf16[16,32,2048]{2,1,0:T(8,128)(2,1)}), bf16[16,32,2048]{2,1,0:T(8,128)(2,1)S(1)}, u32[]{:S(2)}, u32[]{:S(2)}) %all-to-all-start.1) | async-done | bytes 2097184 | tf_op jit(solution)/shard_map/all_to_all | solution.py:132
  160.3 14.1 %scatter_custom_fusion.2 = f32[2048,2048]{1,0:T(8,128)} fusion(s32[512]{0:T(512)S(1)} %get-tuple-element.11, f32[]{:T(128)} %constant.111.clone.1, bf16[512,2048]{1,0:T(8,128)(2,1)S(1)} %bitcast.73, f32[512]{0:T(512)S(1)} %scatter_custom_fusion.1), kind=kCustom, calls=%fused_computation.4 | custom fusion | flops 3145728 | bytes 18876420 | tf_op jit(solution)/shard_map/scatter-add | solution.py:135
  174.4 9.3 %convert_element_type.108 = bf16[2048,2048]{1,0:T(8,128)(2,1)} convert(f32[2048,2048]{1,0:T(8,128)} %scatter_custom_fusion.2) | non-fusion elementwise | flops 4194304 | bytes 25165824 | tf_op jit(solution)/shard_map/convert_element_type | solution.py:138
  183.7 0.0 reduce-scatter.2.cloned.1.call-update
  183.8 1.0 copy-done.4
  184.8 0.2 fusion.34
  185.0 0.0 all-gather.5.cloned.1.call-done
  185.0 2.1 convolution_convert_fusion.1
  187.1 2.2 collective-permute-start
  189.3 5.4 %collective-permute-done = bf16[15,512]{1,0:T(8,128)(2,1)S(1)} collective-permute-done((bf16[15,512]{1,0:T(8,128)(2,1)S(1)}, bf16[15,512]{1,0:T(8,128)(2,1)S(1)}, u32[]{:S(2)}, u32[]{:S(2)}) %collective-permute-start) | collective-permute-done | bytes 15392 | tf_op jit(solution)/shard_map/ppermute | solution.py:16
  194.8 0.1 fusion.82
  194.8 0.1 pad.4
  194.9 0.4 fusion.43
  195.4 0.0 copy-start.9
  195.4 0.1 copy.22
  195.6 0.1 fusion.78
  195.7 0.5 copy-done.11
  196.2 0.2 fusion.60
  196.5 0.1 fusion.55
  196.6 0.0 all-gather.7.cloned.1.call-done
  196.6 2.9 convolution_convert_fusion
  199.6 12.7 %all-gather.11.cloned.1.call-done = bf16[768,6144]{1,0:T(8,128)(2,1)} async-done(((bf16[48,6144]{1,0:T(8,128)(2,1)}), bf16[768,6144]{1,0:T(8,128)(2,1)}) %all-gather.11.cloned.1.call-update) | async-done | bytes 9437200 | tf_op jit(solution)/shard_map/all_gather | solution.py:22
  212.3 3.1 %fusion.6 = f32[128,768]{1,0:T(8,128)S(1)} fusion(bf16[128,2048]{1,0:T(8,128)(2,1)S(1)} %copy-done.3, bf16[768,6144]{1,0:T(8,128)(2,1)} %all-gather.11.cloned.1.call-done), kind=kOutput, calls=%fused_computation.11 | convolution fusion | flops 402653184 | bytes 4063232 | tf_op jit(solution)/shard_map/dot_general | solution.py:44
  215.3 68.5 %reduce-scatter.2.cloned.1.call-done = bf16[128,2048]{1,0:T(8,128)(2,1)} async-done(((bf16[2048,2048]{1,0:T(8,128)(2,1)}), bf16[128,2048]{1,0:T(8,128)(2,1)}) %reduce-scatter.2.cloned.1.call-update) | async-done | bytes 524304 | tf_op jit(solution)/shard_map/reduce_scatter | solution.py:137
  283.9 6.1 %fusion.20 = bf16[128,2048]{1,0:T(8,128)(2,1)} fusion(bf16[768,6144]{1,0:T(8,128)(2,1)} %all-gather.11.cloned.1.call-done, bf16[128,2048]{1,0:T(8,128)(2,1)} %fusion.39, bf16[128,2048]{1,0:T(8,128)(2,1)} %reduce-scatter.2.cloned.1.call-done, f32[128,768]{1,0:T(8,128)S(1)} %fusion.6), kind=kOutput, calls=%fused_computation.21 | convolution fusion | flops 806682624 | bytes 8257536 | tf_op jit(solution)/shard_map/dot_general | solution.py:141
  (42 shorter events, 0.3 us)
Async XLA Ops:
  7.2 113.1 %copy-start = (bf16[1,768,2048]{2,1,0:T(8,128)(2,1)S(1)}, bf16[1,768,2048]{2,1,0:T(8,128)(2,1)}, u32[]{:S(2)}) copy-start(bf16[1,768,2048]{2,1,0:T(8,128)(2,1)} %param.28) | copy-start | bytes 9437188
  7.2 5.1 %copy-start.6 = (bf16[48,2048]{1,0:T(8,128)(2,1)S(1)}, bf16[48,2048]{1,0:T(8,128)(2,1)}, u32[]{:S(2)}) copy-start(bf16[48,2048]{1,0:T(8,128)(2,1)} %param.30) | copy-start | bytes 589828
  7.2 5.1 %copy-start.5 = (bf16[48,2048]{1,0:T(8,128)(2,1)S(1)}, bf16[48,2048]{1,0:T(8,128)(2,1)}, u32[]{:S(2)}) copy-start(bf16[48,2048]{1,0:T(8,128)(2,1)} %param.31) | copy-start | bytes 589828
  7.2 6.9 %copy-start.8 = (s32[2048,2]{0,1:T(2,128)S(1)}, s32[2048,2]{0,1:T(2,128)}, u32[]{:S(2)}) copy-start(s32[2048,2]{0,1:T(2,128)} %param.24) | copy-start | bytes 49156
  7.2 62.4 %all-gather.9.cloned.1.call-start = ((), (), s32[]{:S(2)}) async-start(), calls=%async_computation.5 | async-start | bytes 8912896 | tf_op jit(solution)/shard_map/all_gather | solution.py:168
  10.7 174.3 %all-gather.5.cloned.1.call-start = ((), (), s32[]{:S(2)}) async-start(), calls=%async_computation.3 | async-start | bytes 2228224 | tf_op jit(solution)/shard_map/all_gather | solution.py:166
  11.5 185.2 %all-gather.7.cloned.1.call-start = ((), (), s32[]{:S(2)}) async-start(), calls=%async_computation.4 | async-start | bytes 2228224 | tf_op jit(solution)/shard_map/all_gather | solution.py:167
  12.2 200.1 %all-gather.11.cloned.1.call-start = ((), (), s32[]{:S(2)}) async-start(), calls=%async_computation.7 | async-start | bytes 10027008 | tf_op jit(solution)/shard_map/all_gather | solution.py:22
  81.2 36.1 %copy-start.10 = (bf16[1,2048,768]{2,1,0:T(8,128)(2,1)S(1)}, bf16[1,2048,768]{2,1,0:T(8,128)(2,1)}, u32[]{:S(2)}) copy-start(bf16[1,2048,768]{2,1,0:T(8,128)(2,1)} %param.26) | copy-start | bytes 9437188
  116.0 1.3 copy-start.2
  128.7 5.1 %copy-start.7 = (bf16[2048,2]{0,1:T(2,128)(2,1)S(1)}, bf16[2048,2]{0,1:T(2,128)(2,1)}, u32[]{:S(2)}) copy-start(bf16[2048,2]{0,1:T(2,128)(2,1)} %param.25) | copy-start | bytes 24580
  128.7 31.7 %all-to-all-start.1 = ((bf16[16,32,2048]{2,1,0:T(8,128)(2,1)}), bf16[16,32,2048]{2,1,0:T(8,128)(2,1)S(1)}, u32[]{:S(2)}, u32[]{:S(2)}) async-start(bf16[16,32,2048]{2,1,0:T(8,128)(2,1)} %bitcast.78), calls=%async_computation.1 | async-start | bytes 4194304 | tf_op jit(solution)/shard_map/all_to_all | solution.py:132
  133.7 150.2 %reduce-scatter.2.cloned.1.call-start = ((), (), s32[]{:S(2)}) async-start(), calls=%async_computation.6 | async-start | bytes 8912896 | tf_op jit(solution)/shard_map/reduce_scatter | solution.py:137
  183.7 1.0 copy-start.4
  183.7 1.3 copy-start.12
  187.1 7.6 %collective-permute-start = (bf16[15,512]{1,0:T(8,128)(2,1)S(1)}, bf16[15,512]{1,0:T(8,128)(2,1)S(1)}, u32[]{:S(2)}, u32[]{:S(2)}) collective-permute-start(bf16[15,512]{1,0:T(8,128)(2,1)S(1)} %slice.81), channel_id=1, source_target_pairs={{0,1},{1,2},{2,3},{3,4},{4,5},{5,6},{6,7},{7,8},{8,9},{9,10},{10,1... | collective-permute-start | bytes 46088 | tf_op jit(solution)/shard_map/ppermute | solution.py:16
  195.3 0.9 copy-start.11
  195.4 1.1 copy-start.9
  195.7 16.5 %copy-start.3 = (bf16[128,2048]{1,0:T(8,128)(2,1)S(1)}, bf16[128,2048]{1,0:T(8,128)(2,1)}, u32[]{:S(2)}) copy-start(bf16[128,2048]{1,0:T(8,128)(2,1)} %fusion.39) | copy-start | bytes 1572868
  283.9 6.1 %copy-start.1 = (bf16[1,768,2048]{2,1,0:T(8,128)(2,1)S(1)}, bf16[1,768,2048]{2,1,0:T(8,128)(2,1)}, u32[]{:S(2)}) copy-start(bf16[1,768,2048]{2,1,0:T(8,128)(2,1)} %param.28) | copy-start | bytes 9437188
Sparse Core Ops, SparseCore 0:
  10.8 58.7 all-gather.8
  71.5 37.9 all-gather.4
  111.3 39.0 all-gather.6
  152.1 60.1 all-gather.10
  214.7 69.1 reduce-scatter.1
where the time goes:
time: 298 us; the launch traced here: 297 us
  waiting for transfers between devices  121 us (41%)
  local copies, waits for them, and re-layouts  52.1 us (17%)
  other arithmetic  41.4 us (14%)
  blocking collectives  34.8 us (12%)
  matrix products  25.8 us (9%)
  between operations  14.2 us (5%)
  starting transfers between devices  7.43 us (2%)
    reduce_scatter x1, waiting for transfers between devices, expert_half(): lax.psum_scatter(routed.astype(jnp.bfloat16), 'tp', scatter_dimension=0,...  68.5 us
    all_to_all x1, blocking collectives, expert_half(): lax.all_to_all(outgoing, 'ep', split_axis=0, concat_axis=0, tiled=True)  34.8 us
    all_gather x1, waiting for transfers between devices, shards(): lax.all_gather(moe_normed, 'tp', axis=0, tiled=True)  22.9 us
    scatter x1, local copies, waits for them, and re-layouts, expert_half(): jnp.zeros((ep_count * capacity,), jnp.float32).at[slot_index]  15.7 us
    scatter x1, local copies, waits for them, and re-layouts, expert_half(): slot_token = jnp.full((ep_count * capacity,), block_rows, jnp.int32).at[s...  15.5 us
    scatter-add x1, other arithmetic, expert_half(): jnp.zeros((block_rows, model_width), jnp.float32).at[slot_token]  14.1 us
    all_gather x1, waiting for transfers between devices, sent_together(): whole = lax.all_gather(both, axis, axis=dim, tiled=True)  12.7 us
    all_to_all x1, waiting for transfers between devices, expert_half(): lax.all_to_all(results, 'ep', split_axis=0, concat_axis=0, tiled=True)  9.91 us
  transfers between devices with their start and end apart: 7, of which 5 were waited for; matrix products, arithmetic and copies ran while one was open for 36% of the time, Pallas kernels for 0%

commit v1 on v0

v1 whole, which is shorter than its diff:
```python
import functools

import jax
import jax.numpy as jnp
from jax import lax
from jax.experimental import pallas as pl
from jax.experimental.pallas import tpu as pltpu
from jax.sharding import PartitionSpec as P

NORM_EPS = 1e-06
ROUTED_SCALE = 2.5
MESH = pl.DeviceIdType.MESH
F32 = jnp.float32
BF16 = jnp.bfloat16
HALO = 16
LANES = 128
MIX_AT = 4

NT = (((1,), (1,)), ((), ()))


def dot(a, b):
    return jnp.dot(a, b, preferred_element_type=F32)


def rms_rows(values, gain):
    floats = values.astype(F32)
    scaled = floats * lax.rsqrt(jnp.mean(floats * floats, axis=-1, keepdims=True) + NORM_EPS)
    return (scaled * gain).astype(BF16)


def kernel(
    n_ep, n_tp, n_chunks, cap,
    moe_in, moe_gain, routes, score, mix_gain, pool_mat, pool_scale,
    mix_in, mix_w_in, mix_w_out, exp_gate, exp_up, exp_down, sh_gate, sh_up, sh_down,
    mixed_ref, moe_ref,
    g_buf, out_buf, in_buf, res_buf, ret_buf, sib_buf, up_buf, dn_buf,
    p_mat, s_mat, spread, hid, hid_acc, gate_acc, up_acc, hidden,
    wg, wu, wd, sgu, sd, mx, wi, wo, pool_buf,
    local_sem, ag_send, ag_up, ag_dn, ag_sib, disp_send, disp_recv, ret_send, ret_recv,
    rs_send, rs_sib, rs_up, rs_dn, w_send, w_recv,
):
    tokens, width = moe_in.shape
    cols = width // n_chunks
    n_z = n_tp // 2
    half = tokens // 2
    slots = n_ep * cap
    ff = wd.shape[0]
    n_sh = sh_gate.shape[0]
    ep = lax.axis_index("ep")
    tp = lax.axis_index("tp")
    z = tp // 2
    k = tp % 2
    lin = ep * n_tp + tp

    def at_z(steps):
        return {"tp": ((z + steps + n_z) % n_z) * 2 + k}

    up, dn, sib = at_z(1), at_z(-1), {"tp": z * 2 + 1 - k}

    def ep_peer(offset):
        return {"ep": (ep + offset) % n_ep}

    after = lax.rem(lin + 1, n_ep * n_tp)
    before = lax.rem(lin + n_ep * n_tp - 1, n_ep * n_tp)

    def by_lin(index):
        return {"ep": index // n_tp, "tp": index % n_tp}

    def send(src, dst, send_sem, recv_sem, device):
        pltpu.make_async_remote_copy(
            src_ref=src, dst_ref=dst, send_sem=send_sem, recv_sem=recv_sem,
            device_id=device, device_id_type=MESH,
        ).start()

    def got(ref, sem):
        pltpu.make_async_remote_copy(
            src_ref=ref, dst_ref=ref, send_sem=sem, recv_sem=sem,
            device_id=sib, device_id_type=MESH,
        ).wait_recv()

    def sent(ref, sem):
        pltpu.make_async_remote_copy(
            src_ref=ref, dst_ref=ref, send_sem=sem, recv_sem=sem,
            device_id=sib, device_id_type=MESH,
        ).wait_send()

    barrier = pltpu.get_barrier_semaphore()

    def hello(device):
        pl.semaphore_signal(barrier, inc=1, device_id=device, device_id_type=MESH)

    for steps in range(1, n_z):
        hello(at_z(steps))
    hello(sib)
    hello(by_lin(after))
    hello(by_lin(before))

    @pl.loop(1, n_ep)
    def _(o):
        hello(ep_peer(o))

    q_rows = pl.ds(pl.multiple_of((ep % 4) * 32, 32), 32)
    q_grp = ep // 4
    e_rows = pl.ds(pl.multiple_of(ep * 32, 32), 32)
    loads = [
        pltpu.make_async_copy(
            mix_w_in.at[q_rows, pl.ds(pl.multiple_of(q_grp * LANES, LANES), LANES)],
            wi.at[q_grp, z, k, q_rows, :], local_sem.at[0]),
        pltpu.make_async_copy(mix_w_out.at[e_rows, :], wo.at[z, k, e_rows, :], local_sem.at[1]),
        pltpu.make_async_copy(sh_gate, sgu.at[pl.ds(0, n_sh), :], local_sem.at[2]),
        pltpu.make_async_copy(sh_up, sgu.at[pl.ds(LANES, n_sh), :], local_sem.at[3]),
        pltpu.make_async_copy(sh_down, sd.at[pl.ds(0, n_sh), :], local_sem.at[4]),
        pltpu.make_async_copy(exp_gate.at[0], wg, local_sem.at[5]),
        pltpu.make_async_copy(exp_up.at[0], wu, local_sem.at[6]),
        pltpu.make_async_copy(exp_down.at[0], wd, local_sem.at[7]),
        pltpu.make_async_copy(mix_in, mx.at[pl.ds(HALO, tokens), :], local_sem.at[8]),
    ]
    for load in loads:
        load.start()

    normed = rms_rows(moe_in[...], moe_gain[...])
    for f in range(n_chunks):
        g_buf[f, tp] = normed[:, f * cols:(f + 1) * cols]

    pl.semaphore_wait(barrier, n_z - 1 + 3 + n_ep - 1)

    send(mix_in.at[pl.ds(tokens - HALO, HALO), :], mx.at[pl.ds(0, HALO), :],
         w_send.at[0], w_recv.at[0], by_lin(after))

    def own_pieces(f):
        own = g_buf.at[f, tp]
        send(own, own, ag_send.at[f, 0], ag_up.at[f, 0], up)
        send(own, own, ag_send.at[f, 1], ag_dn.at[f, 0], dn)
        send(own, own, ag_send.at[f, 2], ag_sib.at[f], sib)

    loads[0].wait()
    loads[1].wait()
    wi_own = wi.at[q_grp, z, k, q_rows, :]
    wo_own = wo.at[z, k, e_rows, :]
    for steps in range(1, n_z):
        send(wi_own, wi_own, w_send.at[1], w_recv.at[1], at_z(steps))
        send(wo_own, wo_own, w_send.at[1], w_recv.at[1], at_z(steps))

    def gather_step(i):
        @pl.when(i < n_chunks)
        def _():
            own_pieces(i)

        for hop in range(1, 4):
            f = i - hop

            @pl.when((f >= 0) & (f < n_chunks))
            def _():
                from_dn = g_buf.at[f, ((z - hop + n_z) % n_z) * 2 + k]
                got(from_dn, ag_up.at[f, hop - 1])
                part = from_dn if hop < 3 else from_dn.at[pl.ds(0, half), :]
                send(part, part, ag_send.at[f, 0], ag_up.at[f, hop], up)
                from_up = g_buf.at[f, ((z + hop) % n_z) * 2 + k]
                got(from_up, ag_dn.at[f, hop - 1])
                part2 = from_up if hop < 3 else from_up.at[pl.ds(half, half), :]
                send(part2, part2, ag_send.at[f, 1], ag_dn.at[f, hop], dn)
                send(from_dn, from_dn, ag_send.at[f, 2], ag_sib.at[f], sib)
                send(from_up, from_up, ag_send.at[f, 2], ag_sib.at[f], sib)

        f4 = i - 4

        @pl.when((f4 >= 0) & (f4 < n_chunks))
        def _():
            far = g_buf.at[f4, ((z + 4) % n_z) * 2 + k]
            got(far.at[pl.ds(0, half), :], ag_up.at[f4, 3])
            got(far.at[pl.ds(half, half), :], ag_dn.at[f4, 3])
            send(far, far, ag_send.at[f4, 2], ag_sib.at[f4], sib)

    own_rows = pl.ds(pl.multiple_of(ep * cap, cap), cap)

    def dispatch(f):
        got(g_buf.at[f, pl.ds(0, n_z)], ag_sib.at[f])
        rows_all = g_buf[f].reshape(n_tp * tokens, cols)
        tile = slots // 2

        @pl.loop(0, 2)
        def _(m):
            rows = pl.ds(pl.multiple_of(m * tile, tile), tile)
            out_buf[f, rows, :] = dot(p_mat[rows, :], rows_all).astype(BF16)

        @pl.loop(1, n_ep)
        def _(o):
            to = lax.rem(ep + o, n_ep)
            send(out_buf.at[f, pl.ds(pl.multiple_of(to * cap, cap), cap), :],
                 in_buf.at[f, own_rows, :], disp_send.at[f], disp_recv.at[f], {"ep": to})

        in_buf[f, own_rows, :] = out_buf[f, own_rows, :]

    def shared_up_part(f):
        at = pl.ds(pl.multiple_of(f * cols, cols), cols)
        w = sgu[:, at]

        @pl.loop(0, n_tp // 4)
        def _(m):
            x = g_buf[f, pl.ds(m * 4, 4)].reshape(4 * tokens, cols)
            rows = pl.ds(pl.multiple_of(m * 4 * tokens, 4 * tokens), 4 * tokens)
            part = lax.dot_general(x, w, NT, preferred_element_type=F32)

            @pl.when(f == 0)
            def _():
                hid_acc[rows, :] = part

            @pl.when(f > 0)
            def _():
                hid_acc[rows, :] += part

    def expert_up_part(f):
        got(in_buf.at[f, pl.ds(0, slots - cap), :], disp_recv.at[f])
        at = pl.ds(pl.multiple_of(f * cols, cols), cols)
        tile = slots // 2
        for w, acc in ((wg, gate_acc), (wu, up_acc)):
            @pl.loop(0, 2)
            def _(m):
                rows = pl.ds(pl.multiple_of(m * tile, tile), tile)
                part = dot(in_buf[f, rows, :], w[at, :])

                @pl.when(f == 0)
                def _():
                    acc[rows, :] = part

                @pl.when(f > 0)
                def _():
                    acc[rows, :] += part

    def route_tables():
        lane = lax.broadcasted_iota(jnp.int32, (LANES, slots), 1)
        row = lax.broadcasted_iota(jnp.int32, (LANES, slots), 0)
        spread[0] = (row == lane // cap).astype(BF16)
        spread[1] = (row - n_ep == lane // cap).astype(BF16)
        wants = (lax.broadcasted_iota(jnp.int32, (tokens, slots), 1) % cap).astype(F32)
        rank_of = lax.broadcasted_iota(jnp.int32, (n_ep, cap, tokens), 1).astype(F32)
        ahead = (lax.broadcasted_iota(jnp.int32, (tokens, tokens), 0)
                 < lax.broadcasted_iota(jnp.int32, (tokens, tokens), 1)).astype(BF16)
        named = lax.broadcasted_iota(jnp.int32, (n_ep, tokens), 0) * n_tp + tp

        def block(b, taken):
            at = pl.ds(pl.multiple_of(b * tokens, tokens), tokens)
            pair = routes[:, at]
            marks = score[:, at].astype(F32)
            total = marks[0:1] + marks[1:2]
            first = pair[0:1] == named
            second = pair[1:2] == named
            mine = first | second
            flags = mine.astype(F32)
            place = dot(flags.astype(BF16), ahead) + taken
            code = jnp.where(mine, place, -1.0)
            weight = jnp.where(first, marks[0:1] / total * ROUTED_SCALE,
                               jnp.where(second, marks[1:2] / total * ROUTED_SCALE, 0.0))
            hot = (code[:, None, :] == rank_of).astype(BF16)
            p_mat[:, at] = hot.reshape(slots, tokens)
            both = jnp.concatenate(
                [code, weight, jnp.zeros((LANES - 2 * n_ep, tokens), F32)], axis=0)
            turned = both.T.astype(BF16)
            ranks = dot(turned, spread[0])
            scale = dot(turned, spread[1])
            spot = (b % 2) * n_z + b // 2
            s_mat[pl.ds(pl.multiple_of(spot * tokens, tokens), tokens), :] = jnp.where(
                ranks == wants, scale, 0.0).astype(BF16)
            return taken + jnp.sum(flags, axis=1, keepdims=True)

        lax.fori_loop(0, n_tp, block, jnp.zeros((n_ep, 1), F32))

    gather_step(0)
    sgu[n_sh:LANES, :] = jnp.zeros((LANES - n_sh, width), BF16)
    sgu[LANES + n_sh:, :] = jnp.zeros((LANES - n_sh, width), BF16)
    sd[n_sh:, :] = jnp.zeros((LANES - n_sh, width), BF16)
    gather_step(1)
    route_tables()
    for load in loads[2:]:
        load.wait()

    wi_set = wi.at[q_grp, :, k, q_rows, :]
    wo_set = wo.at[:, k, e_rows, :]

    @pl.loop(2, n_chunks + 7)
    def _(i):
        gather_step(i)

        @pl.when(i == 2)
        def _():
            got(wo.at[pl.ds(0, n_z - 1), 0, pl.ds(0, 64), :], w_recv.at[1])

            @pl.loop(1, n_ep)
            def _(o):
                send(wi_set, wi_set, w_send.at[2], w_recv.at[2], ep_peer(o))
                send(wo_set, wo_set, w_send.at[3], w_recv.at[3], ep_peer(o))

        f5 = i - 5

        @pl.when((f5 >= 0) & (f5 < n_chunks))
        def _():
            dispatch(f5)
            shared_up_part(f5)

        f6 = i - 7

        @pl.when(f6 >= 0)
        def _():
            expert_up_part(f6)

    @pl.loop(0, 4)
    def _(m):
        tile = slots // 4
        rows = pl.ds(pl.multiple_of(m * tile, tile), tile)
        hidden[rows, :] = (jax.nn.silu(gate_acc[rows, :]) * up_acc[rows, :]).astype(BF16)

    def shared_hidden():
        @pl.loop(0, n_tp)
        def _(b):
            rows = pl.ds(pl.multiple_of(b * tokens, tokens), tokens)
            spot = (b % 2) * n_z + b // 2
            both = hid_acc[rows, :]
            hid[pl.ds(pl.multiple_of(spot * tokens, tokens), tokens), :] = (
                jax.nn.silu(both[:, :LANES]) * both[:, LANES:]).astype(BF16)

    def expert_down(f):
        at = pl.ds(pl.multiple_of(f * cols, cols), cols)
        tile = slots // 2

        @pl.loop(0, 2)
        def _(m):
            rows = pl.ds(pl.multiple_of(m * tile, tile), tile)
            res_buf[f, rows, :] = dot(hidden[rows, :], wd[:, at]).astype(BF16)

        @pl.loop(1, n_ep)
        def _(o):
            to = lax.rem(ep + o, n_ep)
            send(res_buf.at[f, pl.ds(pl.multiple_of(to * cap, cap), cap), :],
                 ret_buf.at[f, own_rows, :], ret_send.at[f], ret_recv.at[f], {"ep": to})

        ret_buf[f, own_rows, :] = res_buf[f, own_rows, :]

    def combine(f):
        got(ret_buf.at[f, pl.ds(0, slots - cap), :], ret_recv.at[f])
        at = pl.ds(pl.multiple_of(f * cols, cols), cols)
        back = ret_buf[f]
        down = sd[:, at]

        @pl.loop(0, n_tp // 2)
        def _(m):
            rows = pl.ds(pl.multiple_of(m * 2 * tokens, 2 * tokens), 2 * tokens)
            part = dot(s_mat[rows, :], back) + dot(hid[rows, :], down)
            g_buf[f, pl.ds(m * 2, 2)] = part.astype(BF16).reshape(2, tokens, cols)

        send(g_buf.at[f, pl.ds((1 - k) * n_z, n_z)], sib_buf.at[f],
             rs_send.at[f, 2], rs_sib.at[f], sib)

    def spot_of(steps):
        return (z + steps + n_z) % n_z

    def plus(f, place, rows, other):
        here = g_buf[f, k * n_z + place, rows, :].astype(F32) + other.astype(F32)
        g_buf[f, k * n_z + place, rows, :] = here.astype(BF16)

    every = pl.ds(0, tokens)
    low = pl.ds(0, half)
    high = pl.ds(half, half)

    def scatter_step(i):
        f = i - 6

        @pl.when((f >= 0) & (f < n_chunks))
        def _():
            got(up_buf.at[f, 3], rs_up.at[f, 3])
            got(dn_buf.at[f, 3], rs_dn.at[f, 3])
            at = pl.ds(pl.multiple_of(f * cols, cols), cols)
            moe_ref[:, at] = (g_buf[f, k * n_z + z].astype(F32) + up_buf[f, 3].astype(F32)
                              + dn_buf[f, 3].astype(F32)).astype(BF16)

        for hop in (3, 2, 1):
            f = i - 2 - hop

            @pl.when((f >= 0) & (f < n_chunks))
            def _():
                rows_up = low if hop == 1 else every
                rows_dn = high if hop == 1 else every
                u, d = spot_of(4 - hop), spot_of(hop - 4)
                got(up_buf.at[f, hop - 1, rows_up, :], rs_up.at[f, hop - 1])
                plus(f, u, rows_up, up_buf[f, hop - 1, rows_up, :])
                send(g_buf.at[f, k * n_z + u], up_buf.at[f, hop],
                     rs_send.at[f, 0], rs_up.at[f, hop], up)
                got(dn_buf.at[f, hop - 1, rows_dn, :], rs_dn.at[f, hop - 1])
                plus(f, d, rows_dn, dn_buf[f, hop - 1, rows_dn, :])
                send(g_buf.at[f, k * n_z + d], dn_buf.at[f, hop],
                     rs_send.at[f, 1], rs_dn.at[f, hop], dn)

        f2 = i - 2

        @pl.when((f2 >= 0) & (f2 < n_chunks))
        def _():
            got(sib_buf.at[f2], rs_sib.at[f2])
            far = spot_of(4)
            plus(f2, far, every, sib_buf[f2, far])
            send(g_buf.at[f2, k * n_z + far, low, :], up_buf.at[f2, 0, low, :],
                 rs_send.at[f2, 0], rs_up.at[f2, 0], up)
            send(g_buf.at[f2, k * n_z + far, high, :], dn_buf.at[f2, 0, high, :],
                 rs_send.at[f2, 1], rs_dn.at[f2, 0], dn)

            @pl.loop(5, n_z + 4)
            def _(s):
                place = lax.rem(z + s, n_z)
                plus(f2, place, every, sib_buf[f2, place])

    def mixer():
        got(wi.at[:, :, 1 - k], w_recv.at[4])
        got(wo.at[:, 1 - k], w_recv.at[5])
        got(mx.at[pl.ds(0, HALO), :], w_recv.at[0])
        rows = rms_rows(mx[...], mix_gain[...])
        position = lin * tokens + lax.broadcasted_iota(jnp.int32, (tokens, LANES), 0)
        inside = (lax.broadcasted_iota(jnp.int32, (tokens + HALO, LANES), 0) >= HALO) | (lin > 0)
        for g in range(4):
            w = wi[g].reshape(width, LANES)
            projected = dot(rows, w).astype(BF16).astype(F32)
            projected = jnp.where(inside, projected, 0.0)
            run = projected
            for step in range(g + 1):
                run = run + pltpu.roll(run, 2 ** step, 0)
            counts = jnp.minimum(position + 1, 2 ** (g + 1)).astype(F32)
            pooled = run[HALO:] / counts - projected[HALO:]
            grouped = dot(pooled.astype(BF16), pool_mat[g])
            pool_buf[:, g * LANES:(g + 1) * LANES] = (
                grouped * pool_scale[:, g * LANES:(g + 1) * LANES]).astype(BF16)

        @pl.loop(0, n_tp)
        def _(t):
            at = pl.ds(pl.multiple_of(t * LANES, LANES), LANES)
            mixed_ref[:, at] = dot(pool_buf[...], wo[t // 2, t % 2]).astype(BF16)

    def return_step(i):
        @pl.when(i < n_chunks)
        def _():
            expert_down(i)

    def combine_step(i):
        f1 = i - 1

        @pl.when((f1 >= 0) & (f1 < n_chunks))
        def _():
            combine(f1)

    return_step(0)
    for f in range(n_chunks):
        sent(g_buf.at[f, pl.ds(0, n_z - 1), pl.ds(0, half), :], ag_send.at[f, 0])
        sent(g_buf.at[f, pl.ds(0, n_z - 1), pl.ds(0, half), :], ag_send.at[f, 1])
        sent(g_buf.at[f, pl.ds(0, n_z)], ag_send.at[f, 2])
    shared_hidden()

    @pl.loop(1, n_chunks + 6)
    def _(i):
        return_step(i)
        scatter_step(i)
        combine_step(i)

        @pl.when(i == 1)
        def _():
            got(wo.at[:, 0, pl.ds(0, 32 * (n_ep - 1)), :], w_recv.at[2])
            got(wo.at[:, 0, pl.ds(0, 32 * (n_ep - 1)), :], w_recv.at[3])
            send(wi.at[:, :, k], wi.at[:, :, k], w_send.at[4], w_recv.at[4], sib)
            send(wo.at[:, k], wo.at[:, k], w_send.at[5], w_recv.at[5], sib)

        @pl.when(i == MIX_AT)
        def _():
            mixer()

    for f in range(n_chunks):
        sent(out_buf.at[f, pl.ds(0, slots - cap), :], disp_send.at[f])
        sent(res_buf.at[f, pl.ds(0, slots - cap), :], ret_send.at[f])
        sent(g_buf.at[f, pl.ds(0, n_z - 1), pl.ds(0, half), :], rs_send.at[f, 0])
        sent(g_buf.at[f, pl.ds(0, n_z - 1), pl.ds(0, half), :], rs_send.at[f, 1])
        sent(sib_buf.at[f], rs_send.at[f, 2])
    sent(mx.at[pl.ds(0, HALO), :], w_send.at[0])
    sent(wo.at[pl.ds(0, n_z - 1), 0, pl.ds(0, 64), :], w_send.at[1])
    sent(wo.at[:, 0, pl.ds(0, 32 * (n_ep - 1)), :], w_send.at[2])
    sent(wo.at[:, 0, pl.ds(0, 32 * (n_ep - 1)), :], w_send.at[3])
    sent(wi.at[:, :, k], w_send.at[4])
    sent(wo.at[:, k], w_send.at[5])


def shards(
    n_ep, n_tp, n_chunks,
    mix_in, mix_gain, mix_w_in, pool_mat, pool_scale, mix_w_out, moe_in, moe_gain,
    routes, route_score, exp_gate, exp_up, exp_down, shared_gate, shared_up, shared_down,
):
    tokens, width = moe_in.shape
    cap = 2 * routes.shape[0] * routes.shape[1] // (n_ep * n_tp)
    slots = n_ep * cap
    ff = exp_gate.shape[2]
    cols = width // n_chunks
    n_z = n_tp // 2
    vmem = pl.BlockSpec(memory_space=pltpu.VMEM)
    hbm = pl.BlockSpec(memory_space=pl.ANY)
    dma = pltpu.SemaphoreType.DMA
    big = (n_chunks, n_tp, tokens, cols)
    return pl.pallas_call(
        functools.partial(kernel, n_ep, n_tp, n_chunks, cap),
        out_shape=(
            jax.ShapeDtypeStruct((tokens, width), BF16),
            jax.ShapeDtypeStruct((tokens, width), BF16),
        ),
        in_specs=[vmem] * 7 + [hbm] * 9,
        out_specs=(vmem, vmem),
        scratch_shapes=[
            pltpu.VMEM(big, BF16),
            pltpu.VMEM((n_chunks, slots, cols), BF16),
            pltpu.VMEM((n_chunks, slots, cols), BF16),
            pltpu.VMEM((n_chunks, slots, cols), BF16),
            pltpu.VMEM((n_chunks, slots, cols), BF16),
            pltpu.VMEM((n_chunks, n_z, tokens, cols), BF16),
            pltpu.VMEM((n_chunks, 4, tokens, cols), BF16),
            pltpu.VMEM((n_chunks, 4, tokens, cols), BF16),
            pltpu.VMEM((slots, n_tp * tokens), BF16),
            pltpu.VMEM((n_tp * tokens, slots), BF16),
            pltpu.VMEM((2, LANES, slots), BF16),
            pltpu.VMEM((n_tp * tokens, LANES), BF16),
            pltpu.VMEM((n_tp * tokens, 2 * LANES), F32),
            pltpu.VMEM((slots, ff), F32),
            pltpu.VMEM((slots, ff), F32),
            pltpu.VMEM((slots, ff), BF16),
            pltpu.VMEM((width, ff), BF16),
            pltpu.VMEM((width, ff), BF16),
            pltpu.VMEM((ff, width), BF16),
            pltpu.VMEM((2 * LANES, width), BF16),
            pltpu.VMEM((LANES, width), BF16),
            pltpu.VMEM((tokens + HALO, width), BF16),
            pltpu.VMEM((4, n_z, 2, tokens, LANES), BF16),
            pltpu.VMEM((n_z, 2, 4 * LANES, LANES), BF16),
            pltpu.VMEM((tokens, 4 * LANES), BF16),
            dma((9,)),
            dma((n_chunks, 3)),
            dma((n_chunks, 4)),
            dma((n_chunks, 4)),
            dma((n_chunks,)),
            dma((n_chunks,)),
            dma((n_chunks,)),
            dma((n_chunks,)),
            dma((n_chunks,)),
            dma((n_chunks, 3)),
            dma((n_chunks,)),
            dma((n_chunks, 4)),
            dma((n_chunks, 4)),
            dma((6,)),
            dma((6,)),
        ],
        compiler_params=pltpu.CompilerParams(
            collective_id=0, has_side_effects=True, vmem_limit_bytes=67043328
        ),
    )(
        moe_in, moe_gain.reshape(1, width), routes.T, route_score.T,
        mix_gain.reshape(1, width), pool_mat, pool_scale.reshape(1, -1),
        mix_in, mix_w_in, mix_w_out, exp_gate, exp_up, exp_down,
        shared_gate, shared_up, shared_down,
    )


def solution(mesh):
    n_ep, n_tp = mesh.shape["ep"], mesh.shape["tp"]
    return jax.shard_map(
        functools.partial(shards, n_ep, n_tp, 8),
        mesh=mesh,
        in_specs=(
            P(("ep", "tp"), None),
            P(),
            P("tp", None),
            P(),
            P(),
            P(None, "tp"),
            P(("ep", "tp"), None),
            P(),
            P("ep", None),
            P("ep", None),
            P(("ep", "tp"), None, None),
            P(("ep", "tp"), None, None),
            P(("ep", "tp"), None, None),
            P("tp", None),
            P("tp", None),
            P("tp", None),
        ),
        out_specs=(P(("ep", "tp"), None), P(("ep", "tp"), None)),
        check_vma=False,
    )
```

time: 298 us -> 163 us (0.55)
  Pallas kernels: 0 us -> 158 us
  waiting for transfers between devices: 121 us -> 0 us
  local copies, waits for them, and re-layouts: 52.1 us -> 3.76 us
  other arithmetic: 41.4 us -> 0 us
  blocking collectives: 34.8 us -> 0 us
  matrix products: 25.8 us -> 0 us
  between operations: 14.2 us -> 0.65 us
  starting transfers between devices: 7.43 us -> 0 us
    pallas_call x0 -> x1, Pallas kernels: none -> 158 us  [shards(): pl.pallas_call(functools.partial(kernel, n_ep, n_tp, n_chunks, cap), out_...]
    reduce_scatter x1 -> x0, waiting for transfers between devices: 68.5 us -> none  [expert_half(): lax.psum_scatter(routed.astype(jnp.bfloat16), 'tp', scatter_dimension=0,...]
    all_gather x4 -> x0, waiting for transfers between devices: 35.6 us -> none  [the longest x1 22.9 us: shards(): lax.all_gather(moe_normed, 'tp', axis=0, tiled=True)]
    all_to_all x1 -> x0, blocking collectives: 34.8 us -> none  [expert_half(): lax.all_to_all(outgoing, 'ep', split_axis=0, concat_axis=0, tiled=True)]
    scatter x2 -> x0, local copies, waits for them, and re-layouts: 31.2 us -> none  [the longest x1 15.7 us: expert_half(): jnp.zeros((ep_count * capacity,), jnp.float32).at[slot_index]]
    dot_general x7 -> x0, matrix products: 25.8 us -> none  [the longest x1 8.39 us: expert_ffn(): jnp.dot(hidden, w_down, preferred_element_type=jnp.float32)]
    scatter-add x1 -> x0, other arithmetic: 14.1 us -> none  [expert_half(): jnp.zeros((block_rows, model_width), jnp.float32).at[slot_token]]
    convert_element_type x6 -> x0, other arithmetic: 12.2 us -> none  [the longest x1 9.3 us: expert_half(): routed.astype(jnp.bfloat16)]
  transfers between devices with their start and end apart: 7 -> 0, of which waited for: 5 -> 0; matrix products, arithmetic and copies ran while one was open for 36% -> 0% of each run, Pallas kernels for 0% -> 0%
where the time goes in v1:
time: 163 us; the launch traced here: 162 us
  Pallas kernels  158 us (97%)
  local copies, waits for them, and re-layouts  3.76 us (2%)
    pallas_call x1, Pallas kernels, shards(): pl.pallas_call(functools.partial(kernel, n_ep, n_tp, n_chunks, cap), out_...  158 us
    unnamed x2, local copies, waits for them, and re-layouts  3.76 us

profile of v1, /device:TPU:2, one launch (start us, length us, event | category | flops | bytes accessed | tf_op | source)
XLA Modules:
  0.0 162.2 jit_solution(9128882679680246420)
XLA Ops:
  0.6 157.8 %shard_map.167 = (bf16[128,2048]{1,0:T(8,128)(2,1)}, bf16[128,2048]{1,0:T(8,128)(2,1)}) custom-call(bf16[128,2048]{1,0:T(8,128)(2,1)} %moe_in.1, f32[1,2048]{1,0:T(1,128)} %bitcast.6, s32[2,2048]{1,0:T(2,128)} %bitcast.5, bf16[2,2048]{1,0:T(2,128)(2,1)} %bitcast.7, f32[1,2048]{1,0:T(1,128)} %bitcast.8, bf16[4,128,128]{2,1,0:T(8,128)(2,1)} %pool_mat.1, ...), custom_call_target="tpu_custom_call" | custom-call | tf_op jit(solution)/shard_map/pallas_call | solution.py:500
  158.5 1.9 %copy.20 = bf16[128,2048]{1,0:T(8,128)(2,1)} copy(bf16[128,2048]{1,0:T(8,128)(2,1)} %get-tuple-element.4) | data formatting | bytes 1048576
  160.4 1.9 %copy.21 = bf16[128,2048]{1,0:T(8,128)(2,1)} copy(bf16[128,2048]{1,0:T(8,128)(2,1)} %get-tuple-element.5) | data formatting | bytes 1048576

commit v2 on v1

--- a/solution.py
+++ b/solution.py
@@ -14,7 +14,6 @@
 BF16 = jnp.bfloat16
 HALO = 16
 LANES = 128
-MIX_AT = 4
 
 NT = (((1,), (1,)), ((), ()))
 
@@ -31,13 +30,14 @@
 
 def kernel(
     n_ep, n_tp, n_chunks, cap,
-    moe_in, moe_gain, routes, score, mix_gain, pool_mat, pool_scale,
+    moe_in_hbm, moe_gain_hbm, routes_hbm, score_hbm, mix_gain_hbm, pool_mat_hbm, pool_scale_hbm,
     mix_in, mix_w_in, mix_w_out, exp_gate, exp_up, exp_down, sh_gate, sh_up, sh_down,
-    mixed_ref, moe_ref,
+    mixed_hbm, moe_hbm,
+    moe_in, moe_gain, routes, score, mix_gain, pool_mat, pool_scale, mixed_ref, moe_ref, taken_ref,
     g_buf, out_buf, in_buf, res_buf, ret_buf, sib_buf, up_buf, dn_buf,
     p_mat, s_mat, spread, hid, hid_acc, gate_acc, up_acc, hidden,
-    wg, wu, wd, sgu, sd, mx, wi, wo, pool_buf,
-    local_sem, ag_send, ag_up, ag_dn, ag_sib, disp_send, disp_recv, ret_send, ret_recv,
+    wg, wu, wd, sgu, sgt, sd, mx, wi, wo, pool_buf,
+    local_sem, out_sem, ag_send, ag_up, ag_dn, ag_sib, disp_send, disp_recv, ret_send, ret_recv,
     rs_send, rs_sib, rs_up, rs_dn, w_send, w_recv,
 ):
     tokens, width = moe_in.shape
@@ -103,11 +103,19 @@
     q_rows = pl.ds(pl.multiple_of((ep % 4) * 32, 32), 32)
     q_grp = ep // 4
     e_rows = pl.ds(pl.multiple_of(ep * 32, 32), 32)
+    early = [
+        pltpu.make_async_copy(src, dst, local_sem.at[9 + j])
+        for j, (src, dst) in enumerate((
+            (moe_in_hbm, moe_in), (moe_gain_hbm, moe_gain), (routes_hbm, routes),
+            (score_hbm, score), (mix_gain_hbm, mix_gain), (pool_mat_hbm, pool_mat),
+            (pool_scale_hbm, pool_scale)))
+    ]
     loads = [
         pltpu.make_async_copy(
             mix_w_in.at[q_rows, pl.ds(pl.multiple_of(q_grp * LANES, LANES), LANES)],
             wi.at[q_grp, z, k, q_rows, :], local_sem.at[0]),
-        pltpu.make_async_copy(mix_w_out.at[e_rows, :], wo.at[z, k, e_rows, :], local_sem.at[1]),
+        pltpu.make_async_copy(
+            mix_w_out.at[e_rows, :], wo.at[z, k, q_grp, q_rows, :], local_sem.at[1]),
         pltpu.make_async_copy(sh_gate, sgu.at[pl.ds(0, n_sh), :], local_sem.at[2]),
         pltpu.make_async_copy(sh_up, sgu.at[pl.ds(LANES, n_sh), :], local_sem.at[3]),
         pltpu.make_async_copy(sh_down, sd.at[pl.ds(0, n_sh), :], local_sem.at[4]),
@@ -116,17 +124,14 @@
         pltpu.make_async_copy(exp_down.at[0], wd, local_sem.at[7]),
         pltpu.make_async_copy(mix_in, mx.at[pl.ds(HALO, tokens), :], local_sem.at[8]),
     ]
-    for load in loads:
+    for load in early + loads:
         load.start()
+    for load in early:
+        load.wait()
 
     normed = rms_rows(moe_in[...], moe_gain[...])
     for f in range(n_chunks):
         g_buf[f, tp] = normed[:, f * cols:(f + 1) * cols]
-
-    pl.semaphore_wait(barrier, n_z - 1 + 3 + n_ep - 1)
-
-    send(mix_in.at[pl.ds(tokens - HALO, HALO), :], mx.at[pl.ds(0, HALO), :],
-         w_send.at[0], w_recv.at[0], by_lin(after))
 
     def own_pieces(f):
         own = g_buf.at[f, tp]
@@ -134,13 +139,50 @@
         send(own, own, ag_send.at[f, 1], ag_dn.at[f, 0], dn)
         send(own, own, ag_send.at[f, 2], ag_sib.at[f], sib)
 
-    loads[0].wait()
-    loads[1].wait()
     wi_own = wi.at[q_grp, z, k, q_rows, :]
-    wo_own = wo.at[z, k, e_rows, :]
-    for steps in range(1, n_z):
-        send(wi_own, wi_own, w_send.at[1], w_recv.at[1], at_z(steps))
-        send(wo_own, wo_own, w_send.at[1], w_recv.at[1], at_z(steps))
+    wo_own = wo.at[z, k, q_grp, q_rows, :]
+    x_at, y_at = ep % 4, ep // 4
+
+    def weights_along_z():
+        send(mix_in.at[pl.ds(tokens - HALO, HALO), :], mx.at[pl.ds(0, HALO), :],
+             w_send.at[0], w_recv.at[0], by_lin(after))
+        loads[0].wait()
+        loads[1].wait()
+        for steps in range(1, n_z):
+            send(wi_own, wi_own, w_send.at[1], w_recv.at[1], at_z(steps))
+            send(wo_own, wo_own, w_send.at[1], w_recv.at[1], at_z(steps))
+
+    def along_x(steps):
+        return {"ep": y_at * 4 + (x_at + steps) % 4}
+
+    def along_y(steps):
+        return {"ep": ((y_at + steps) % 4) * 4 + x_at}
+
+    wi_set = wi.at[q_grp, :, k, q_rows, :]
+    wo_set = wo.at[:, k, q_grp, q_rows, :]
+    wi_row = wi.at[q_grp, :, k]
+    wo_col = wo.at[:, k, :, q_rows, :]
+    three = wo.at[:, 0, 0, pl.ds(0, 96), :]
+    three_rows = wo.at[:, 0, pl.ds(0, 3)]
+
+    def weights_first():
+        got(wo.at[pl.ds(0, n_z - 1), 0, 0, pl.ds(0, 64), :], w_recv.at[1])
+        for steps in range(1, 4):
+            send(wi_set, wi_set, w_send.at[2], w_recv.at[2], along_x(steps))
+            send(wo_set, wo_set, w_send.at[3], w_recv.at[3], along_y(steps))
+
+    def weights_second():
+        got(three, w_recv.at[2])
+        got(three, w_recv.at[3])
+        for steps in range(1, 4):
+            send(wi_row, wi_row, w_send.at[6], w_recv.at[6], along_y(steps))
+            send(wo_col, wo_col, w_send.at[7], w_recv.at[7], along_x(steps))
+
+    def weights_sibling():
+        got(three_rows, w_recv.at[6])
+        got(three_rows, w_recv.at[7])
+        send(wi.at[:, :, k], wi.at[:, :, k], w_send.at[4], w_recv.at[4], sib)
+        send(wo.at[:, k], wo.at[:, k], w_send.at[5], w_recv.at[5], sib)
 
     def gather_step(i):
         @pl.when(i < n_chunks)
@@ -177,12 +219,7 @@
     def dispatch(f):
         got(g_buf.at[f, pl.ds(0, n_z)], ag_sib.at[f])
         rows_all = g_buf[f].reshape(n_tp * tokens, cols)
-        tile = slots // 2
-
-        @pl.loop(0, 2)
-        def _(m):
-            rows = pl.ds(pl.multiple_of(m * tile, tile), tile)
-            out_buf[f, rows, :] = dot(p_mat[rows, :], rows_all).astype(BF16)
+        out_buf[f] = dot(p_mat[...], rows_all).astype(BF16)
 
         @pl.loop(1, n_ep)
         def _(o):
@@ -192,47 +229,41 @@
 
         in_buf[f, own_rows, :] = out_buf[f, own_rows, :]
 
-    def shared_up_part(f):
-        at = pl.ds(pl.multiple_of(f * cols, cols), cols)
-        w = sgu[:, at]
+    def shared_up(first):
+        base = 0 if first else n_chunks // 2
 
         @pl.loop(0, n_tp // 4)
         def _(m):
-            x = g_buf[f, pl.ds(m * 4, 4)].reshape(4 * tokens, cols)
+            x = jnp.concatenate(
+                [g_buf[base + f, pl.ds(m * 4, 4)].reshape(4 * tokens, cols)
+                 for f in range(n_chunks // 2)], axis=1)
             rows = pl.ds(pl.multiple_of(m * 4 * tokens, 4 * tokens), 4 * tokens)
-            part = lax.dot_general(x, w, NT, preferred_element_type=F32)
-
-            @pl.when(f == 0)
-            def _():
+            part = dot(x, sgt[base * cols:(base + n_chunks // 2) * cols, :])
+            if first:
                 hid_acc[rows, :] = part
-
-            @pl.when(f > 0)
-            def _():
-                hid_acc[rows, :] += part
+            else:
+                both = hid_acc[rows, :] + part
+                units = (jax.nn.silu(both[:, :LANES]) * both[:, LANES:]).astype(BF16)
+                for q in range(4):
+                    spot = (q % 2) * n_z + m * 2 + q // 2
+                    hid[pl.ds(pl.multiple_of(spot * tokens, tokens), tokens), :] = (
+                        units[q * tokens:(q + 1) * tokens])
 
     def expert_up_part(f):
         got(in_buf.at[f, pl.ds(0, slots - cap), :], disp_recv.at[f])
         at = pl.ds(pl.multiple_of(f * cols, cols), cols)
-        tile = slots // 2
         for w, acc in ((wg, gate_acc), (wu, up_acc)):
-            @pl.loop(0, 2)
-            def _(m):
-                rows = pl.ds(pl.multiple_of(m * tile, tile), tile)
-                part = dot(in_buf[f, rows, :], w[at, :])
-
-                @pl.when(f == 0)
-                def _():
-                    acc[rows, :] = part
-
-                @pl.when(f > 0)
-                def _():
-                    acc[rows, :] += part
-
-    def route_tables():
-        lane = lax.broadcasted_iota(jnp.int32, (LANES, slots), 1)
-        row = lax.broadcasted_iota(jnp.int32, (LANES, slots), 0)
-        spread[0] = (row == lane // cap).astype(BF16)
-        spread[1] = (row - n_ep == lane // cap).astype(BF16)
+            part = dot(in_buf[f], w[at, :])
+
+            @pl.when(f == 0)
+            def _():
+                acc[...] = part
+
+            @pl.when(f > 0)
+            def _():
+                acc[...] += part
+
+    def route_tables(b_from, b_to):
         wants = (lax.broadcasted_iota(jnp.int32, (tokens, slots), 1) % cap).astype(F32)
         rank_of = lax.broadcasted_iota(jnp.int32, (n_ep, cap, tokens), 1).astype(F32)
         ahead = (lax.broadcasted_iota(jnp.int32, (tokens, tokens), 0)
@@ -264,45 +295,56 @@
                 ranks == wants, scale, 0.0).astype(BF16)
             return taken + jnp.sum(flags, axis=1, keepdims=True)
 
-        lax.fori_loop(0, n_tp, block, jnp.zeros((n_ep, 1), F32))
-
+        taken = lax.fori_loop(b_from, b_to, block, taken_ref[:, :1])
+        taken_ref[...] = jnp.broadcast_to(taken, taken_ref.shape)
+
+    pl.semaphore_wait(barrier, n_z - 1 + 3 + n_ep - 1)
     gather_step(0)
+    weights_along_z()
+    lane = lax.broadcasted_iota(jnp.int32, (LANES, slots), 1)
+    row = lax.broadcasted_iota(jnp.int32, (LANES, slots), 0)
+    spread[0] = (row == lane // cap).astype(BF16)
+    spread[1] = (row - n_ep == lane // cap).astype(BF16)
+    taken_ref[...] = jnp.zeros_like(taken_ref)
     sgu[n_sh:LANES, :] = jnp.zeros((LANES - n_sh, width), BF16)
     sgu[LANES + n_sh:, :] = jnp.zeros((LANES - n_sh, width), BF16)
     sd[n_sh:, :] = jnp.zeros((LANES - n_sh, width), BF16)
-    gather_step(1)
-    route_tables()
     for load in loads[2:]:
         load.wait()
-
-    wi_set = wi.at[q_grp, :, k, q_rows, :]
-    wo_set = wo.at[:, k, e_rows, :]
-
-    @pl.loop(2, n_chunks + 7)
+    for f in range(n_chunks):
+        sgt[f * cols:(f + 1) * cols, :] = sgu[:, f * cols:(f + 1) * cols].T
+
+    @pl.loop(1, n_chunks + 7)
     def _(i):
         gather_step(i)
 
         @pl.when(i == 2)
         def _():
-            got(wo.at[pl.ds(0, n_z - 1), 0, pl.ds(0, 64), :], w_recv.at[1])
-
-            @pl.loop(1, n_ep)
-            def _(o):
-                send(wi_set, wi_set, w_send.at[2], w_recv.at[2], ep_peer(o))
-                send(wo_set, wo_set, w_send.at[3], w_recv.at[3], ep_peer(o))
+            weights_first()
+
+        @pl.when(i == 4)
+        def _():
+            weights_second()
+
+        @pl.when(i < 5)
+        def _():
+            route_tables((i - 1) * (n_tp // 4), i * (n_tp // 4))
 
         f5 = i - 5
 
         @pl.when((f5 >= 0) & (f5 < n_chunks))
         def _():
             dispatch(f5)
-            shared_up_part(f5)
 
         f6 = i - 7
 
         @pl.when(f6 >= 0)
         def _():
             expert_up_part(f6)
+
+        @pl.when(i == n_chunks // 2 + 4)
+        def _():
+            shared_up(True)
 
     @pl.loop(0, 4)
     def _(m):
@@ -310,23 +352,9 @@
         rows = pl.ds(pl.multiple_of(m * tile, tile), tile)
         hidden[rows, :] = (jax.nn.silu(gate_acc[rows, :]) * up_acc[rows, :]).astype(BF16)
 
-    def shared_hidden():
-        @pl.loop(0, n_tp)
-        def _(b):
-            rows = pl.ds(pl.multiple_of(b * tokens, tokens), tokens)
-            spot = (b % 2) * n_z + b // 2
-            both = hid_acc[rows, :]
-            hid[pl.ds(pl.multiple_of(spot * tokens, tokens), tokens), :] = (
-                jax.nn.silu(both[:, :LANES]) * both[:, LANES:]).astype(BF16)
-
     def expert_down(f):
         at = pl.ds(pl.multiple_of(f * cols, cols), cols)
-        tile = slots // 2
-
-        @pl.loop(0, 2)
-        def _(m):
-            rows = pl.ds(pl.multiple_of(m * tile, tile), tile)
-            res_buf[f, rows, :] = dot(hidden[rows, :], wd[:, at]).astype(BF16)
+        res_buf[f] = dot(hidden[...], wd[:, at]).astype(BF16)
 
         @pl.loop(1, n_ep)
         def _(o):
@@ -342,14 +370,20 @@
         back = ret_buf[f]
         down = sd[:, at]
 
-        @pl.loop(0, n_tp // 2)
-        def _(m):
-            rows = pl.ds(pl.multiple_of(m * 2 * tokens, 2 * tokens), 2 * tokens)
-            part = dot(s_mat[rows, :], back) + dot(hid[rows, :], down)
-            g_buf[f, pl.ds(m * 2, 2)] = part.astype(BF16).reshape(2, tokens, cols)
-
+        def half_of(core):
+            @pl.loop(0, 2)
+            def _(j):
+                m = core * 2 + j
+                many = n_z // 2 * tokens
+                rows = pl.ds(pl.multiple_of(m * many, many), many)
+                part = dot(s_mat[rows, :], back) + dot(hid[rows, :], down)
+                g_buf[f, pl.ds(m * (n_z // 2), n_z // 2)] = (
+                    part.astype(BF16).reshape(n_z // 2, tokens, cols))
+
+        half_of(1 - k)
         send(g_buf.at[f, pl.ds((1 - k) * n_z, n_z)], sib_buf.at[f],
              rs_send.at[f, 2], rs_sib.at[f], sib)
+        half_of(k)
 
     def spot_of(steps):
         return (z + steps + n_z) % n_z
@@ -372,6 +406,7 @@
             at = pl.ds(pl.multiple_of(f * cols, cols), cols)
             moe_ref[:, at] = (g_buf[f, k * n_z + z].astype(F32) + up_buf[f, 3].astype(F32)
                               + dn_buf[f, 3].astype(F32)).astype(BF16)
+            pltpu.make_async_copy(moe_ref.at[:, at], moe_hbm.at[:, at], out_sem.at[0]).start()
 
         for hop in (3, 2, 1):
             f = i - 2 - hop
@@ -407,66 +442,66 @@
                 place = lax.rem(z + s, n_z)
                 plus(f2, place, every, sib_buf[f2, place])
 
-    def mixer():
+    def mixer_norm():
         got(wi.at[:, :, 1 - k], w_recv.at[4])
         got(wo.at[:, 1 - k], w_recv.at[5])
         got(mx.at[pl.ds(0, HALO), :], w_recv.at[0])
-        rows = rms_rows(mx[...], mix_gain[...])
+        mx[...] = rms_rows(mx[...], mix_gain[...])
+
+    def mixer_group(g):
         position = lin * tokens + lax.broadcasted_iota(jnp.int32, (tokens, LANES), 0)
         inside = (lax.broadcasted_iota(jnp.int32, (tokens + HALO, LANES), 0) >= HALO) | (lin > 0)
-        for g in range(4):
-            w = wi[g].reshape(width, LANES)
-            projected = dot(rows, w).astype(BF16).astype(F32)
-            projected = jnp.where(inside, projected, 0.0)
-            run = projected
-            for step in range(g + 1):
-                run = run + pltpu.roll(run, 2 ** step, 0)
-            counts = jnp.minimum(position + 1, 2 ** (g + 1)).astype(F32)
-            pooled = run[HALO:] / counts - projected[HALO:]
-            grouped = dot(pooled.astype(BF16), pool_mat[g])
-            pool_buf[:, g * LANES:(g + 1) * LANES] = (
-                grouped * pool_scale[:, g * LANES:(g + 1) * LANES]).astype(BF16)
-
-        @pl.loop(0, n_tp)
+        projected = dot(mx[...], wi[g].reshape(width, LANES)).astype(BF16).astype(F32)
+        projected = jnp.where(inside, projected, 0.0)
+        run = projected
+        for step in range(g + 1):
+            run = run + pltpu.roll(run, 2 ** step, 0)
+        counts = jnp.minimum(position + 1, 2 ** (g + 1)).astype(F32)
+        pooled = run[HALO:] / counts - projected[HALO:]
+        grouped = dot(pooled.astype(BF16), pool_mat[g])
+        pool_buf[:, g * LANES:(g + 1) * LANES] = (
+            grouped * pool_scale[:, g * LANES:(g + 1) * LANES]).astype(BF16)
+
+    def mixer_out(part):
+        @pl.loop(part * (n_tp // 4), (part + 1) * (n_tp // 4))
         def _(t):
             at = pl.ds(pl.multiple_of(t * LANES, LANES), LANES)
-            mixed_ref[:, at] = dot(pool_buf[...], wo[t // 2, t % 2]).astype(BF16)
-
-    def return_step(i):
-        @pl.when(i < n_chunks)
-        def _():
-            expert_down(i)
-
-    def combine_step(i):
-        f1 = i - 1
-
-        @pl.when((f1 >= 0) & (f1 < n_chunks))
-        def _():
-            combine(f1)
-
-    return_step(0)
+            w = wo[t // 2, t % 2].reshape(4 * LANES, LANES)
+            mixed_ref[:, at] = dot(pool_buf[...], w).astype(BF16)
+
+        cut = width // 4
+        at = pl.ds(pl.multiple_of(part * cut, cut), cut)
+        pltpu.make_async_copy(mixed_ref.at[:, at], mixed_hbm.at[:, at], out_sem.at[1]).start()
+
+    expert_down(0)
     for f in range(n_chunks):
         sent(g_buf.at[f, pl.ds(0, n_z - 1), pl.ds(0, half), :], ag_send.at[f, 0])
         sent(g_buf.at[f, pl.ds(0, n_z - 1), pl.ds(0, half), :], ag_send.at[f, 1])
         sent(g_buf.at[f, pl.ds(0, n_z)], ag_send.at[f, 2])
-    shared_hidden()
+    expert_down(1)
+    shared_up(False)
+    expert_down(2)
+    weights_sibling()
 
     @pl.loop(1, n_chunks + 6)
     def _(i):
-        return_step(i)
         scatter_step(i)
-        combine_step(i)
-
-        @pl.when(i == 1)
-        def _():
-            got(wo.at[:, 0, pl.ds(0, 32 * (n_ep - 1)), :], w_recv.at[2])
-            got(wo.at[:, 0, pl.ds(0, 32 * (n_ep - 1)), :], w_recv.at[3])
-            send(wi.at[:, :, k], wi.at[:, :, k], w_send.at[4], w_recv.at[4], sib)
-            send(wo.at[:, k], wo.at[:, k], w_send.at[5], w_recv.at[5], sib)
-
-        @pl.when(i == MIX_AT)
-        def _():
-            mixer()
+
+        @pl.when(i <= n_chunks)
+        def _():
+            combine(i - 1)
+
+        @pl.when(i + 2 < n_chunks)
+        def _():
+            expert_down(i + 2)
+
+        pl.when(i == n_chunks - 4)(mixer_norm)
+        for g in range(4):
+            pl.when(i == n_chunks - 3 + g)(functools.partial(mixer_group, g))
+
+        @pl.when((i > n_chunks) & (i <= n_chunks + 4))
+        def _():
+            mixer_out(i - n_chunks - 1)
 
     for f in range(n_chunks):
         sent(out_buf.at[f, pl.ds(0, slots - cap), :], disp_send.at[f])
@@ -475,9 +510,13 @@
         sent(g_buf.at[f, pl.ds(0, n_z - 1), pl.ds(0, half), :], rs_send.at[f, 1])
         sent(sib_buf.at[f], rs_send.at[f, 2])
     sent(mx.at[pl.ds(0, HALO), :], w_send.at[0])
-    sent(wo.at[pl.ds(0, n_z - 1), 0, pl.ds(0, 64), :], w_send.at[1])
-    sent(wo.at[:, 0, pl.ds(0, 32 * (n_ep - 1)), :], w_send.at[2])
-    sent(wo.at[:, 0, pl.ds(0, 32 * (n_ep - 1)), :], w_send.at[3])
+    sent(wo.at[pl.ds(0, n_z - 1), 0, 0, pl.ds(0, 64), :], w_send.at[1])
+    sent(three, w_send.at[2])
+    sent(three, w_send.at[3])
+    sent(three_rows, w_send.at[6])
+    sent(three_rows, w_send.at[7])
+    pltpu.make_async_copy(moe_ref, moe_hbm, out_sem.at[0]).wait()
+    pltpu.make_async_copy(mixed_ref, mixed_hbm, out_sem.at[1]).wait()
     sent(wi.at[:, :, k], w_send.at[4])
     sent(wo.at[:, k], w_send.at[5])
 
@@ -493,7 +532,6 @@
     ff = exp_gate.shape[2]
     cols = width // n_chunks
     n_z = n_tp // 2
-    vmem = pl.BlockSpec(memory_space=pltpu.VMEM)
     hbm = pl.BlockSpec(memory_space=pl.ANY)
     dma = pltpu.SemaphoreType.DMA
     big = (n_chunks, n_tp, tokens, cols)
@@ -503,9 +541,19 @@
             jax.ShapeDtypeStruct((tokens, width), BF16),
             jax.ShapeDtypeStruct((tokens, width), BF16),
         ),
-        in_specs=[vmem] * 7 + [hbm] * 9,
-        out_specs=(vmem, vmem),
+        in_specs=[hbm] * 16,
+        out_specs=(hbm, hbm),
         scratch_shapes=[
+            pltpu.VMEM((tokens, width), BF16),
+            pltpu.VMEM((1, width), F32),
+            pltpu.VMEM((2, routes.shape[0]), jnp.int32),
+            pltpu.VMEM((2, routes.shape[0]), BF16),
+            pltpu.VMEM((1, width), F32),
+            pltpu.VMEM(pool_mat.shape, BF16),
+            pltpu.VMEM((1, pool_scale.shape[0]), F32),
+            pltpu.VMEM((tokens, width), BF16),
+            pltpu.VMEM((tokens, width), BF16),
+            pltpu.VMEM((n_ep, LANES), F32),
             pltpu.VMEM(big, BF16),
             pltpu.VMEM((n_chunks, slots, cols), BF16),
             pltpu.VMEM((n_chunks, slots, cols), BF16),
@@ -526,12 +574,14 @@
             pltpu.VMEM((width, ff), BF16),
             pltpu.VMEM((ff, width), BF16),
             pltpu.VMEM((2 * LANES, width), BF16),
+            pltpu.VMEM((width, 2 * LANES), BF16),
             pltpu.VMEM((LANES, width), BF16),
             pltpu.VMEM((tokens + HALO, width), BF16),
             pltpu.VMEM((4, n_z, 2, tokens, LANES), BF16),
-            pltpu.VMEM((n_z, 2, 4 * LANES, LANES), BF16),
+            pltpu.VMEM((n_z, 2, 4, LANES, LANES), BF16),
             pltpu.VMEM((tokens, 4 * LANES), BF16),
-            dma((9,)),
+            dma((16,)),
+            dma((2,)),
             dma((n_chunks, 3)),
             dma((n_chunks, 4)),
             dma((n_chunks, 4)),
@@ -544,8 +594,8 @@
             dma((n_chunks,)),
             dma((n_chunks, 4)),
             dma((n_chunks, 4)),
-            dma((6,)),
-            dma((6,)),
+            dma((8,)),
+            dma((8,)),
         ],
         compiler_params=pltpu.CompilerParams(
             collective_id=0, has_side_effects=True, vmem_limit_bytes=67043328

time: 163 us -> 139 us (0.85)
  Pallas kernels: 158 us -> 134 us
    pallas_call x1, Pallas kernels: 158 us -> 134 us  [shards(): pl.pallas_call(functools.partial(kernel, n_ep, n_tp, n_chunks, cap), out_...]
where the time goes in v2:
time: 139 us; the launch traced here: 138 us
  Pallas kernels  134 us (96%)
  local copies, waits for them, and re-layouts  3.76 us (3%)
    pallas_call x1, Pallas kernels, shards(): pl.pallas_call(functools.partial(kernel, n_ep, n_tp, n_chunks, cap), out_...  134 us
    unnamed x2, local copies, waits for them, and re-layouts  3.76 us

profile of v2, /device:TPU:2, one launch (start us, length us, event | category | flops | bytes accessed | tf_op | source)
XLA Modules:
  0.0 138.2 jit_solution(1042549651004706889)
XLA Ops:
  0.6 133.8 %shard_map.167 = (bf16[128,2048]{1,0:T(8,128)(2,1)}, bf16[128,2048]{1,0:T(8,128)(2,1)}) custom-call(bf16[128,2048]{1,0:T(8,128)(2,1)} %moe_in_hbm.1, f32[1,2048]{1,0:T(1,128)} %bitcast.6, s32[2,2048]{1,0:T(2,128)} %bitcast.5, bf16[2,2048]{1,0:T(2,128)(2,1)} %bitcast.7, f32[1,2048]{1,0:T(1,128)} %bitcast.8, bf16[4,128,128]{2,1,0:T(8,128)(2,1)} %pool_mat_hbm.1, ...), custom_call_target="tpu_custom_call" | custom-call | tf_op jit(solution)/shard_map/pallas_call | solution.py:538
  134.4 1.9 %copy.20 = bf16[128,2048]{1,0:T(8,128)(2,1)} copy(bf16[128,2048]{1,0:T(8,128)(2,1)} %get-tuple-element.4) | data formatting | bytes 1048576
  136.3 1.9 %copy.21 = bf16[128,2048]{1,0:T(8,128)(2,1)} copy(bf16[128,2048]{1,0:T(8,128)(2,1)} %get-tuple-element.5) | data formatting | bytes 1048576

commit v3 on v2

--- a/solution.py
+++ b/solution.py
@@ -15,7 +15,7 @@
 HALO = 16
 LANES = 128
 
-NT = (((1,), (1,)), ((), ()))
+LOOK = 1
 
 
 def dot(a, b):
@@ -32,12 +32,12 @@
     n_ep, n_tp, n_chunks, cap,
     moe_in_hbm, moe_gain_hbm, routes_hbm, score_hbm, mix_gain_hbm, pool_mat_hbm, pool_scale_hbm,
     mix_in, mix_w_in, mix_w_out, exp_gate, exp_up, exp_down, sh_gate, sh_up, sh_down,
-    mixed_hbm, moe_hbm,
-    moe_in, moe_gain, routes, score, mix_gain, pool_mat, pool_scale, mixed_ref, moe_ref, taken_ref,
+    mixed_ref, moe_ref,
+    moe_in, moe_gain, routes, score, mix_gain, pool_mat, pool_scale, taken_ref,
     g_buf, out_buf, in_buf, res_buf, ret_buf, sib_buf, up_buf, dn_buf,
     p_mat, s_mat, spread, hid, hid_acc, gate_acc, up_acc, hidden,
     wg, wu, wd, sgu, sgt, sd, mx, wi, wo, pool_buf,
-    local_sem, out_sem, ag_send, ag_up, ag_dn, ag_sib, disp_send, disp_recv, ret_send, ret_recv,
+    local_sem, ag_send, ag_up, ag_dn, ag_sib, disp_send, disp_recv, ret_send, ret_recv,
     rs_send, rs_sib, rs_up, rs_dn, w_send, w_recv,
 ):
     tokens, width = moe_in.shape
@@ -126,7 +126,7 @@
     ]
     for load in early + loads:
         load.start()
-    for load in early:
+    for load in early[:2]:
         load.wait()
 
     normed = rms_rows(moe_in[...], moe_gain[...])
@@ -144,10 +144,6 @@
     x_at, y_at = ep % 4, ep // 4
 
     def weights_along_z():
-        send(mix_in.at[pl.ds(tokens - HALO, HALO), :], mx.at[pl.ds(0, HALO), :],
-             w_send.at[0], w_recv.at[0], by_lin(after))
-        loads[0].wait()
-        loads[1].wait()
         for steps in range(1, n_z):
             send(wi_own, wi_own, w_send.at[1], w_recv.at[1], at_z(steps))
             send(wo_own, wo_own, w_send.at[1], w_recv.at[1], at_z(steps))
@@ -185,9 +181,9 @@
         send(wo.at[:, k], wo.at[:, k], w_send.at[5], w_recv.at[5], sib)
 
     def gather_step(i):
-        @pl.when(i < n_chunks)
-        def _():
-            own_pieces(i)
+        @pl.when(i + LOOK < n_chunks)
+        def _():
+            own_pieces(i + LOOK)
 
         for hop in range(1, 4):
             f = i - hop
@@ -216,14 +212,14 @@
 
     own_rows = pl.ds(pl.multiple_of(ep * cap, cap), cap)
 
+    others = [(ep + step) % n_ep for step in range(1, n_ep)]
+
     def dispatch(f):
         got(g_buf.at[f, pl.ds(0, n_z)], ag_sib.at[f])
         rows_all = g_buf[f].reshape(n_tp * tokens, cols)
         out_buf[f] = dot(p_mat[...], rows_all).astype(BF16)
 
-        @pl.loop(1, n_ep)
-        def _(o):
-            to = lax.rem(ep + o, n_ep)
+        for to in others:
             send(out_buf.at[f, pl.ds(pl.multiple_of(to * cap, cap), cap), :],
                  in_buf.at[f, own_rows, :], disp_send.at[f], disp_recv.at[f], {"ep": to})
 
@@ -299,8 +295,13 @@
         taken_ref[...] = jnp.broadcast_to(taken, taken_ref.shape)
 
     pl.semaphore_wait(barrier, n_z - 1 + 3 + n_ep - 1)
+    for f in range(LOOK):
+        own_pieces(f)
     gather_step(0)
-    weights_along_z()
+    loads[0].wait()
+    loads[1].wait()
+    send(mix_in.at[pl.ds(tokens - HALO, HALO), :], mx.at[pl.ds(0, HALO), :],
+         w_send.at[0], w_recv.at[0], by_lin(after))
     lane = lax.broadcasted_iota(jnp.int32, (LANES, slots), 1)
     row = lax.broadcasted_iota(jnp.int32, (LANES, slots), 0)
     spread[0] = (row == lane // cap).astype(BF16)
@@ -309,7 +310,7 @@
     sgu[n_sh:LANES, :] = jnp.zeros((LANES - n_sh, width), BF16)
     sgu[LANES + n_sh:, :] = jnp.zeros((LANES - n_sh, width), BF16)
     sd[n_sh:, :] = jnp.zeros((LANES - n_sh, width), BF16)
-    for load in loads[2:]:
+    for load in early[2:] + loads[2:]:
         load.wait()
     for f in range(n_chunks):
         sgt[f * cols:(f + 1) * cols, :] = sgu[:, f * cols:(f + 1) * cols].T
@@ -317,14 +318,8 @@
     @pl.loop(1, n_chunks + 7)
     def _(i):
         gather_step(i)
-
-        @pl.when(i == 2)
-        def _():
-            weights_first()
-
-        @pl.when(i == 4)
-        def _():
-            weights_second()
+        pl.when(i == n_chunks + 2)(weights_along_z)
+        pl.when(i == n_chunks + 5)(weights_first)
 
         @pl.when(i < 5)
         def _():
@@ -336,15 +331,15 @@
         def _():
             dispatch(f5)
 
+        @pl.when(i == n_chunks + 4)
+        def _():
+            shared_up(True)
+
         f6 = i - 7
 
         @pl.when(f6 >= 0)
         def _():
             expert_up_part(f6)
-
-        @pl.when(i == n_chunks // 2 + 4)
-        def _():
-            shared_up(True)
 
     @pl.loop(0, 4)
     def _(m):
@@ -356,9 +351,7 @@
         at = pl.ds(pl.multiple_of(f * cols, cols), cols)
         res_buf[f] = dot(hidden[...], wd[:, at]).astype(BF16)
 
-        @pl.loop(1, n_ep)
-        def _(o):
-            to = lax.rem(ep + o, n_ep)
+        for to in others:
             send(res_buf.at[f, pl.ds(pl.multiple_of(to * cap, cap), cap), :],
                  ret_buf.at[f, own_rows, :], ret_send.at[f], ret_recv.at[f], {"ep": to})
 
@@ -406,7 +399,6 @@
             at = pl.ds(pl.multiple_of(f * cols, cols), cols)
             moe_ref[:, at] = (g_buf[f, k * n_z + z].astype(F32) + up_buf[f, 3].astype(F32)
                               + dn_buf[f, 3].astype(F32)).astype(BF16)
-            pltpu.make_async_copy(moe_ref.at[:, at], moe_hbm.at[:, at], out_sem.at[0]).start()
 
         for hop in (3, 2, 1):
             f = i - 2 - hop
@@ -469,9 +461,11 @@
             w = wo[t // 2, t % 2].reshape(4 * LANES, LANES)
             mixed_ref[:, at] = dot(pool_buf[...], w).astype(BF16)
 
-        cut = width // 4
-        at = pl.ds(pl.multiple_of(part * cut, cut), cut)
-        pltpu.make_async_copy(mixed_ref.at[:, at], mixed_hbm.at[:, at], out_sem.at[1]).start()
+    def settle(f):
+        sent(res_buf.at[f, pl.ds(0, slots - cap), :], ret_send.at[f])
+        sent(g_buf.at[f, pl.ds(0, n_z - 1), pl.ds(0, half), :], rs_send.at[f, 0])
+        sent(g_buf.at[f, pl.ds(0, n_z - 1), pl.ds(0, half), :], rs_send.at[f, 1])
+        sent(sib_buf.at[f], rs_send.at[f, 2])
 
     expert_down(0)
     for f in range(n_chunks):
@@ -480,8 +474,10 @@
         sent(g_buf.at[f, pl.ds(0, n_z)], ag_send.at[f, 2])
     expert_down(1)
     shared_up(False)
-    expert_down(2)
-    weights_sibling()
+
+    @pl.loop(2, 5)
+    def _(f):
+        expert_down(f)
 
     @pl.loop(1, n_chunks + 6)
     def _(i):
@@ -490,35 +486,52 @@
         @pl.when(i <= n_chunks)
         def _():
             combine(i - 1)
-
-        @pl.when(i + 2 < n_chunks)
-        def _():
-            expert_down(i + 2)
-
-        pl.when(i == n_chunks - 4)(mixer_norm)
-        for g in range(4):
-            pl.when(i == n_chunks - 3 + g)(functools.partial(mixer_group, g))
-
-        @pl.when((i > n_chunks) & (i <= n_chunks + 4))
-        def _():
-            mixer_out(i - n_chunks - 1)
-
-    for f in range(n_chunks):
-        sent(out_buf.at[f, pl.ds(0, slots - cap), :], disp_send.at[f])
-        sent(res_buf.at[f, pl.ds(0, slots - cap), :], ret_send.at[f])
-        sent(g_buf.at[f, pl.ds(0, n_z - 1), pl.ds(0, half), :], rs_send.at[f, 0])
-        sent(g_buf.at[f, pl.ds(0, n_z - 1), pl.ds(0, half), :], rs_send.at[f, 1])
-        sent(sib_buf.at[f], rs_send.at[f, 2])
-    sent(mx.at[pl.ds(0, HALO), :], w_send.at[0])
-    sent(wo.at[pl.ds(0, n_z - 1), 0, 0, pl.ds(0, 64), :], w_send.at[1])
-    sent(three, w_send.at[2])
-    sent(three, w_send.at[3])
-    sent(three_rows, w_send.at[6])
-    sent(three_rows, w_send.at[7])
-    pltpu.make_async_copy(moe_ref, moe_hbm, out_sem.at[0]).wait()
-    pltpu.make_async_copy(mixed_ref, mixed_hbm, out_sem.at[1]).wait()
-    sent(wi.at[:, :, k], w_send.at[4])
-    sent(wo.at[:, k], w_send.at[5])
+            sent(out_buf.at[i - 1, pl.ds(0, slots - cap), :], disp_send.at[i - 1])
+
+        @pl.when(i + 4 < n_chunks)
+        def _():
+            expert_down(i + 4)
+
+        pl.when(i == 3)(weights_second)
+        pl.when(i == n_chunks)(weights_sibling)
+
+        @pl.when(i == n_chunks + 1)
+        def _():
+            mixer_norm()
+            mixer_group(0)
+            mixer_group(1)
+
+        @pl.when(i == n_chunks + 2)
+        def _():
+            mixer_group(2)
+            mixer_group(3)
+            mixer_out(0)
+
+        @pl.when(i == n_chunks + 3)
+        def _():
+            mixer_out(1)
+            mixer_out(2)
+
+        @pl.when(i == n_chunks + 4)
+        def _():
+            mixer_out(3)
+
+        @pl.when(i > 6)
+        def _():
+            settle(i - 7)
+
+        @pl.when(i == n_chunks + 4)
+        def _():
+            sent(mx.at[pl.ds(0, HALO), :], w_send.at[0])
+            sent(wo.at[pl.ds(0, n_z - 1), 0, 0, pl.ds(0, 64), :], w_send.at[1])
+            sent(three, w_send.at[2])
+            sent(three, w_send.at[3])
+            sent(three_rows, w_send.at[6])
+            sent(three_rows, w_send.at[7])
+            sent(wi.at[:, :, k], w_send.at[4])
+            sent(wo.at[:, k], w_send.at[5])
+
+    settle(n_chunks - 1)
 
 
 def shards(
@@ -538,11 +551,11 @@
     return pl.pallas_call(
         functools.partial(kernel, n_ep, n_tp, n_chunks, cap),
         out_shape=(
-            jax.ShapeDtypeStruct((tokens, width), BF16),
-            jax.ShapeDtypeStruct((tokens, width), BF16),
+            pltpu.VMEM((tokens, width), BF16),
+            pltpu.VMEM((tokens, width), BF16),
         ),
         in_specs=[hbm] * 16,
-        out_specs=(hbm, hbm),
+        out_specs=(pl.BlockSpec(memory_space=pltpu.VMEM),) * 2,
         scratch_shapes=[
             pltpu.VMEM((tokens, width), BF16),
             pltpu.VMEM((1, width), F32),
@@ -551,8 +564,6 @@
             pltpu.VMEM((1, width), F32),
             pltpu.VMEM(pool_mat.shape, BF16),
             pltpu.VMEM((1, pool_scale.shape[0]), F32),
-            pltpu.VMEM((tokens, width), BF16),
-            pltpu.VMEM((tokens, width), BF16),
             pltpu.VMEM((n_ep, LANES), F32),
             pltpu.VMEM(big, BF16),
             pltpu.VMEM((n_chunks, slots, cols), BF16),
@@ -581,7 +592,6 @@
             pltpu.VMEM((n_z, 2, 4, LANES, LANES), BF16),
             pltpu.VMEM((tokens, 4 * LANES), BF16),
             dma((16,)),
-            dma((2,)),
             dma((n_chunks, 3)),
             dma((n_chunks, 4)),
             dma((n_chunks, 4)),
@@ -598,7 +608,7 @@
             dma((8,)),
         ],
         compiler_params=pltpu.CompilerParams(
-            collective_id=0, has_side_effects=True, vmem_limit_bytes=67043328
+            collective_id=0, has_side_effects=True, vmem_limit_bytes=60 << 20
         ),
     )(
         moe_in, moe_gain.reshape(1, width), routes.T, route_score.T,

time: 139 us -> 133 us (0.957)
  Pallas kernels: 134 us -> 130 us
  local copies, waits for them, and re-layouts: 3.76 us -> 1.59 us
    pallas_call x1, Pallas kernels: 134 us -> 130 us  [shards(): pl.pallas_call(functools.partial(kernel, n_ep, n_tp, n_chunks, cap), out_...]
    unnamed x2, local copies, waits for them, and re-layouts: 3.76 us -> 1.59 us
where the time goes in v3:
time: 133 us; the launch traced here: 132 us
  Pallas kernels  130 us (98%)
  local copies, waits for them, and re-layouts  1.59 us (1%)
    pallas_call x1, Pallas kernels, shards(): pl.pallas_call(functools.partial(kernel, n_ep, n_tp, n_chunks, cap), out_...  130 us

profile of v3, /device:TPU:2, one launch (start us, length us, event | category | flops | bytes accessed | tf_op | source)
XLA Modules:
  0.0 132.3 jit_solution(15349414039169383740)
XLA Ops:
  0.6 130.1 %shard_map.167 = (bf16[128,2048]{1,0:T(8,128)(2,1)S(1)}, bf16[128,2048]{1,0:T(8,128)(2,1)S(1)}) custom-call(bf16[128,2048]{1,0:T(8,128)(2,1)} %moe_in_hbm.1, f32[1,2048]{1,0:T(1,128)} %bitcast.6, s32[2,2048]{1,0:T(2,128)} %bitcast.5, bf16[2,2048]{1,0:T(2,128)(2,1)} %bitcast.7, f32[1,2048]{1,0:T(1,128)} %bitcast.8, bf16[4,128,128]{2,1,0:T(8,128)(2,1)} %pool_mat_hbm.1, ...), custom_call_target="tpu_custom_call" | custom-call | tf_op jit(solution)/shard_map/pallas_call | solution.py:551
  130.7 0.8 copy.20
  131.5 0.8 copy.21

commit v4 on v3

--- a/solution.py
+++ b/solution.py
@@ -135,8 +135,10 @@
 
     def own_pieces(f):
         own = g_buf.at[f, tp]
-        send(own, own, ag_send.at[f, 0], ag_up.at[f, 0], up)
-        send(own, own, ag_send.at[f, 1], ag_dn.at[f, 0], dn)
+        for q in range(2):
+            part = own.at[pl.ds(q * half, half), :]
+            send(part, part, ag_send.at[f, 0], ag_up.at[f, 0, q], up)
+            send(part, part, ag_send.at[f, 1], ag_dn.at[f, 0, q], dn)
         send(own, own, ag_send.at[f, 2], ag_sib.at[f], sib)
 
     wi_own = wi.at[q_grp, z, k, q_rows, :]
@@ -191,13 +193,16 @@
             @pl.when((f >= 0) & (f < n_chunks))
             def _():
                 from_dn = g_buf.at[f, ((z - hop + n_z) % n_z) * 2 + k]
-                got(from_dn, ag_up.at[f, hop - 1])
-                part = from_dn if hop < 3 else from_dn.at[pl.ds(0, half), :]
-                send(part, part, ag_send.at[f, 0], ag_up.at[f, hop], up)
                 from_up = g_buf.at[f, ((z + hop) % n_z) * 2 + k]
-                got(from_up, ag_dn.at[f, hop - 1])
-                part2 = from_up if hop < 3 else from_up.at[pl.ds(half, half), :]
-                send(part2, part2, ag_send.at[f, 1], ag_dn.at[f, hop], dn)
+                for q in range(2):
+                    part = from_dn.at[pl.ds(q * half, half), :]
+                    got(part, ag_up.at[f, hop - 1, q])
+                    if hop < 3 or q == 0:
+                        send(part, part, ag_send.at[f, 0], ag_up.at[f, hop, q], up)
+                    part = from_up.at[pl.ds(q * half, half), :]
+                    got(part, ag_dn.at[f, hop - 1, q])
+                    if hop < 3 or q == 1:
+                        send(part, part, ag_send.at[f, 1], ag_dn.at[f, hop, q], dn)
                 send(from_dn, from_dn, ag_send.at[f, 2], ag_sib.at[f], sib)
                 send(from_up, from_up, ag_send.at[f, 2], ag_sib.at[f], sib)
 
@@ -206,8 +211,8 @@
         @pl.when((f4 >= 0) & (f4 < n_chunks))
         def _():
             far = g_buf.at[f4, ((z + 4) % n_z) * 2 + k]
-            got(far.at[pl.ds(0, half), :], ag_up.at[f4, 3])
-            got(far.at[pl.ds(half, half), :], ag_dn.at[f4, 3])
+            got(far.at[pl.ds(0, half), :], ag_up.at[f4, 3, 0])
+            got(far.at[pl.ds(half, half), :], ag_dn.at[f4, 3, 1])
             send(far, far, ag_send.at[f4, 2], ag_sib.at[f4], sib)
 
     own_rows = pl.ds(pl.multiple_of(ep * cap, cap), cap)
@@ -390,33 +395,6 @@
     high = pl.ds(half, half)
 
     def scatter_step(i):
-        f = i - 6
-
-        @pl.when((f >= 0) & (f < n_chunks))
-        def _():
-            got(up_buf.at[f, 3], rs_up.at[f, 3])
-            got(dn_buf.at[f, 3], rs_dn.at[f, 3])
-            at = pl.ds(pl.multiple_of(f * cols, cols), cols)
-            moe_ref[:, at] = (g_buf[f, k * n_z + z].astype(F32) + up_buf[f, 3].astype(F32)
-                              + dn_buf[f, 3].astype(F32)).astype(BF16)
-
-        for hop in (3, 2, 1):
-            f = i - 2 - hop
-
-            @pl.when((f >= 0) & (f < n_chunks))
-            def _():
-                rows_up = low if hop == 1 else every
-                rows_dn = high if hop == 1 else every
-                u, d = spot_of(4 - hop), spot_of(hop - 4)
-                got(up_buf.at[f, hop - 1, rows_up, :], rs_up.at[f, hop - 1])
-                plus(f, u, rows_up, up_buf[f, hop - 1, rows_up, :])
-                send(g_buf.at[f, k * n_z + u], up_buf.at[f, hop],
-                     rs_send.at[f, 0], rs_up.at[f, hop], up)
-                got(dn_buf.at[f, hop - 1, rows_dn, :], rs_dn.at[f, hop - 1])
-                plus(f, d, rows_dn, dn_buf[f, hop - 1, rows_dn, :])
-                send(g_buf.at[f, k * n_z + d], dn_buf.at[f, hop],
-                     rs_send.at[f, 1], rs_dn.at[f, hop], dn)
-
         f2 = i - 2
 
         @pl.when((f2 >= 0) & (f2 < n_chunks))
@@ -425,10 +403,48 @@
             far = spot_of(4)
             plus(f2, far, every, sib_buf[f2, far])
             send(g_buf.at[f2, k * n_z + far, low, :], up_buf.at[f2, 0, low, :],
-                 rs_send.at[f2, 0], rs_up.at[f2, 0], up)
+                 rs_send.at[f2, 0], rs_up.at[f2, 0, 0], up)
             send(g_buf.at[f2, k * n_z + far, high, :], dn_buf.at[f2, 0, high, :],
-                 rs_send.at[f2, 1], rs_dn.at[f2, 0], dn)
-
+                 rs_send.at[f2, 1], rs_dn.at[f2, 0, 1], dn)
+
+        for hop in (1, 2, 3):
+            f = i - 2 - hop
+
+            @pl.when((f >= 0) & (f < n_chunks))
+            def _():
+                u, d = spot_of(4 - hop), spot_of(hop - 4)
+
+                def onward(place, buf, sem, way, peer, q):
+                    rows = (low, high)[q]
+                    if hop > 1 or q == way:
+                        got(buf.at[f, hop - 1, rows, :], sem.at[f, hop - 1, q])
+                        plus(f, place, rows, buf[f, hop - 1, rows, :])
+                    send(g_buf.at[f, k * n_z + place, rows, :], buf.at[f, hop, rows, :],
+                         rs_send.at[f, way], sem.at[f, hop, q], peer)
+
+                if hop == 1:
+                    onward(u, up_buf, rs_up, 0, up, 1)
+                    onward(d, dn_buf, rs_dn, 1, dn, 0)
+                    onward(u, up_buf, rs_up, 0, up, 0)
+                    onward(d, dn_buf, rs_dn, 1, dn, 1)
+                else:
+                    for q in range(2):
+                        onward(u, up_buf, rs_up, 0, up, q)
+                        onward(d, dn_buf, rs_dn, 1, dn, q)
+
+        f = i - 6
+
+        @pl.when((f >= 0) & (f < n_chunks))
+        def _():
+            for q, rows in enumerate((low, high)):
+                got(up_buf.at[f, 3, rows, :], rs_up.at[f, 3, q])
+                got(dn_buf.at[f, 3, rows, :], rs_dn.at[f, 3, q])
+            at = pl.ds(pl.multiple_of(f * cols, cols), cols)
+            moe_ref[:, at] = (g_buf[f, k * n_z + z].astype(F32) + up_buf[f, 3].astype(F32)
+                              + dn_buf[f, 3].astype(F32)).astype(BF16)
+
+        @pl.when((f2 >= 0) & (f2 < n_chunks))
+        def _():
             @pl.loop(5, n_z + 4)
             def _(s):
                 place = lax.rem(z + s, n_z)
@@ -593,8 +609,8 @@
             pltpu.VMEM((tokens, 4 * LANES), BF16),
             dma((16,)),
             dma((n_chunks, 3)),
-            dma((n_chunks, 4)),
-            dma((n_chunks, 4)),
+            dma((n_chunks, 4, 2)),
+            dma((n_chunks, 4, 2)),
             dma((n_chunks,)),
             dma((n_chunks,)),
             dma((n_chunks,)),
@@ -602,8 +618,8 @@
             dma((n_chunks,)),
             dma((n_chunks, 3)),
             dma((n_chunks,)),
-            dma((n_chunks, 4)),
-            dma((n_chunks, 4)),
+            dma((n_chunks, 4, 2)),
+            dma((n_chunks, 4, 2)),
             dma((8,)),
             dma((8,)),
         ],

time: 133 us -> 132 us (level)
  Pallas kernels: 130 us -> 128 us
    pallas_call x1, Pallas kernels: 130 us -> 128 us  [shards(): pl.pallas_call(functools.partial(kernel, n_ep, n_tp, n_chunks, cap), out_...]
where the time goes in v4:
time: 132 us; the launch traced here: 130 us
  Pallas kernels  128 us (97%)
  local copies, waits for them, and re-layouts  1.59 us (1%)
    pallas_call x1, Pallas kernels, shards(): pl.pallas_call(functools.partial(kernel, n_ep, n_tp, n_chunks, cap), out_...  128 us

profile of v4, /device:TPU:2, one launch (start us, length us, event | category | flops | bytes accessed | tf_op | source)
XLA Modules:
  0.0 130.3 jit_solution(16005739976493140011)
XLA Ops:
  0.6 128.1 %shard_map.167 = (bf16[128,2048]{1,0:T(8,128)(2,1)S(1)}, bf16[128,2048]{1,0:T(8,128)(2,1)S(1)}) custom-call(bf16[128,2048]{1,0:T(8,128)(2,1)} %moe_in_hbm.1, f32[1,2048]{1,0:T(1,128)} %bitcast.6, s32[2,2048]{1,0:T(2,128)} %bitcast.5, bf16[2,2048]{1,0:T(2,128)(2,1)} %bitcast.7, f32[1,2048]{1,0:T(1,128)} %bitcast.8, bf16[4,128,128]{2,1,0:T(8,128)(2,1)} %pool_mat_hbm.1, ...), custom_call_target="tpu_custom_call" | custom-call | tf_op jit(solution)/shard_map/pallas_call | solution.py:567
  128.7 0.8 copy.20
  129.5 0.8 copy.21
